TPU v7x, 32 devices: a whole 2x2x4 slice. The times are simulated.
32 devices in a mesh: ep: 8 (over z, x), tp: 4 (over y, core).
Axes of the slice: x: 2, y: 2, z: 4, core: 2. Of those that a mesh axis runs over, the one named last changes fastest.
Arguments:
- tokens: bfloat16 [384, 2048], P('ep'), may hold values from -6 to 6
- state: float32 [384, 8, 128, 128], P('ep', 'tp'), may hold values from -4 to 4
- norm_gain: float32 [2048], replicated, may hold values from 0.1 to 1.9
- w_query: bfloat16 [2048, 1024], P('ep', 'tp'), may hold values from -0.125 to 0.125
- w_forget: bfloat16 [2048, 1024], P('ep', 'tp'), may hold values from -0.125 to 0.125
- w_input: bfloat16 [2048, 1024], P('ep', 'tp'), may hold values from -0.125 to 0.125
- w_outgate: bfloat16 [2048, 1024], P('ep', 'tp'), may hold values from -0.125 to 0.125
- lower_bound: float32 [1024], P('tp'), may hold values from 0 to 0.9
- head_gain: float32 [1024], P('tp'), may hold values from 0.1 to 1.9
- w_output: bfloat16 [1024, 2048], P('tp'), may hold values from -0.1875 to 0.1875
- ffn_gain: float32 [2048], replicated, may hold values from 0.1 to 1.9
- route_ids: int32 [384, 4], P('ep'), may hold values from 0 to 15, all different within a row; in each aligned block of 48 rows (0 to 47, 48 to 95, ...) at most 24 rows name the same one
- route_weight: float32 [384, 4], P('ep'), may hold values from 0.2 to 1
- expert_gate: bfloat16 [16, 2048, 1024], P('ep', None, 'tp'), may hold values from -0.125 to 0.125
- expert_up: bfloat16 [16, 2048, 1024], P('ep', None, 'tp'), may hold values from -0.125 to 0.125
- expert_down: bfloat16 [16, 1024, 2048], P('ep', 'tp'), may hold values from -0.1875 to 0.1875
- shared_gate: bfloat16 [2048, 1024], P(None, 'tp'), may hold values from -0.125 to 0.125
- shared_up: bfloat16 [2048, 1024], P(None, 'tp'), may hold values from -0.125 to 0.125
- shared_down: bfloat16 [1024, 2048], P('tp'), may hold values from -0.1875 to 0.1875
- dense_gate: bfloat16 [2048, 8192], P('tp', 'ep'), may hold values from -0.125 to 0.125
- dense_up: bfloat16 [2048, 8192], P('tp', 'ep'), may hold values from -0.125 to 0.125
- dense_down: bfloat16 [8192, 2048], P('ep', 'tp'), may hold values from -0.0625 to 0.0625
- dense_mix: float32 [2048], P('tp'), may hold values from -6 to 6
Outputs:
- mixed: bfloat16 [384, 2048], P('ep', 'tp')
- new_state: float32 [384, 8, 128, 128], P('ep', 'tp')
Inputs may be any that keep to these rules, and one draw needn't show every extreme that they name: `route_ids`: each row names 4 different experts. Among the rows of one device no expert is named more than 24 times, and in every draw some expert is named exactly 24 times by some device's rows.
All inputs are finite; a program needn't handle non-finite values.
Results may differ from a plain program's by a relative error of at most 0.025.
Values may be sent and summed in bfloat16 or wider, within the bound.
A program may use at most 64 MiB of HBM per device.

v0:
```python
import functools

import jax
import jax.numpy as jnp
from jax import lax
from jax.experimental import pallas as pl
from jax.experimental.pallas import tpu as pltpu
from jax.sharding import PartitionSpec as P

EPS = 1e-06
LANES = 128
CORES = 2
F32 = jnp.float32
BF16 = jnp.bfloat16
VMEM_BYTES = 60 * 1024 * 1024


def send(src, dst, sems, slot, peer):
    send_sem, recv_sem = sems
    return pltpu.make_async_remote_copy(
        src_ref=src,
        dst_ref=dst,
        send_sem=send_sem.at[slot],
        recv_sem=recv_sem.at[slot],
        device_id=peer,
        device_id_type=pl.DeviceIdType.MESH,
    )


def span(index, size):
    return pl.ds(pl.multiple_of(index * size, size), size)


def greet(n, tpn, me, tp):
    barrier = pltpu.get_barrier_semaphore()
    for s in range(1, n):
        pl.semaphore_signal(
            barrier,
            inc=1,
            device_id={"ep": lax.rem(me + s, n)},
            device_id_type=pl.DeviceIdType.MESH,
        )
    for s in range(1, tpn):
        pl.semaphore_signal(
            barrier,
            inc=1,
            device_id={"tp": lax.rem(tp + s, tpn)},
            device_id_type=pl.DeviceIdType.MESH,
        )
    pl.semaphore_wait(barrier, n - 1 + tpn - 1)


def front_kernel(n, tpn, move, *refs):
    tokens, gain, route, mix, wq, wf, wi, wo = refs[:8]
    refs = refs[8:]
    if move:
        dgate, dup, ddown = refs[:3]
        refs = refs[3:]
    proj, route_all, mix_all = refs[:3]
    refs = refs[3:]
    if move:
        gate_out, up_out, down_out = refs[:3]
        refs = refs[3:]
    nsend, ncol, psend, precv = refs[:4]
    nsems, rsems, psems, msems = [(refs[4 + 2 * i], refs[5 + 2 * i]) for i in range(4)]
    refs = refs[12:]
    me = lax.axis_index("ep")
    tp = lax.axis_index("tp")
    seq = tokens.shape[0]
    depth = wq.shape[0]
    mixw = wq.shape[1]
    x = tokens[...].astype(F32)
    normed = (
        x * lax.rsqrt(jnp.mean(x * x, axis=-1, keepdims=True) + EPS) * gain[...]
    ).astype(BF16)
    for d in range(n):
        nsend[d] = normed[:, d * depth : (d + 1) * depth]
    greet(n, tpn, me, tp)
    ncopies, others = [None], []
    for s in range(1, n):
        peer = lax.rem(me + s, n)
        copy = send(nsend.at[peer], ncol.at[me], nsems, s, {"ep": peer})
        copy.start()
        ncopies.append(copy)
    if move:
        wsems = (refs[0], refs[1])
        lsems = refs[2]
        rows = dgate.shape[0]
        cols = gate_out.shape[1]
        drows = down_out.shape[0]
        dcols = ddown.shape[1]
        locals_ = []
        for s in range(tpn):
            peer = lax.rem(tp + s, tpn)
            for i, (a, b) in enumerate(
                (
                    (dgate.at[:, span(peer, cols)], gate_out.at[span(tp, rows), :]),
                    (dup.at[:, span(peer, cols)], up_out.at[span(tp, rows), :]),
                    (ddown.at[span(peer, drows), :], down_out.at[:, span(tp, dcols)]),
                )
            ):
                if s == 0:
                    copy = pltpu.make_async_copy(a, b, lsems.at[i])
                    locals_.append(copy)
                else:
                    copy = send(a, b, wsems, i * tpn + s, {"tp": peer})
                    others.append(copy)
                copy.start()
    for s in range(1, tpn):
        copy = send(mix, mix_all.at[tp], msems, s, {"tp": lax.rem(tp + s, tpn)})
        copy.start()
        others.append(copy)
    for s in range(1, n):
        copy = send(route, route_all.at[me], rsems, s, {"ep": lax.rem(me + s, n)})
        copy.start()
        others.append(copy)
    mix_all[tp] = mix[...]
    route_all[me] = route[...]

    def project(block):
        return [
            jnp.dot(block, w[...], preferred_element_type=F32).astype(BF16)
            for w in (wq, wf, wi, wo)
        ]

    pcopies = [None]
    for s in range(1, n):
        source = lax.rem(me + n - s, n)
        ncopies[s].wait_recv()
        for i, part in enumerate(project(ncol[source])):
            psend[source, :, i * mixw : (i + 1) * mixw] = part
        copy = send(psend.at[source], precv.at[me], psems, s, {"ep": source})
        copy.start()
        pcopies.append(copy)
    own = jnp.concatenate(project(nsend[me]), axis=1).astype(F32)
    for s in range(1, n):
        pcopies[s].wait_recv()
        own = own + precv[lax.rem(me + s, n)].astype(F32)
    proj[...] = own.astype(BF16)
    for s in range(1, n):
        ncopies[s].wait_send()
        pcopies[s].wait_send()
    for copy in others:
        copy.wait()
    if move:
        for copy in locals_:
            copy.wait()


def gather_kernel(
    n, tpn, tokens, gain, head, wout, resid, moe, hsend, hrecv, sqsend, sqrecv, *sems
):
    hsems, qsems, esems, ysems, csems = [(sems[2 * i], sems[2 * i + 1]) for i in range(5)]
    me = lax.axis_index("ep")
    tp = lax.axis_index("tp")
    seq, width = tokens.shape
    cols = width // tpn
    side, core = lax.div(tp, CORES), lax.rem(tp, CORES)
    sides = tpn // CORES
    twin = side * CORES + (CORES - 1 - core)
    for t in range(tpn):
        hsend[t] = jnp.dot(
            head[...], wout[:, t * cols : (t + 1) * cols], preferred_element_type=F32
        ).astype(BF16)
    greet(n, tpn, me, tp)
    hcopies = []
    for s in range(1, tpn):
        peer = lax.rem(tp + s, tpn)
        copy = send(hsend.at[peer], hrecv.at[tp], hsems, s, {"tp": peer})
        copy.start()
        hcopies.append(copy)
    total = hsend[tp].astype(F32)
    for s in range(1, tpn):
        hcopies[s - 1].wait_recv()
        total = total + hrecv[lax.rem(tp + tpn - s, tpn)].astype(F32)
    mine = span(tp, cols)
    total = tokens[:, mine].astype(F32) + total
    resid[...] = total
    square = jnp.broadcast_to(jnp.sum(total * total, axis=-1, keepdims=True), (seq, LANES))
    sqsend[...] = square
    qcopies = []
    for s in range(1, tpn):
        copy = send(sqsend, sqrecv.at[tp], qsems, s, {"tp": lax.rem(tp + s, tpn)})
        copy.start()
        qcopies.append(copy)
    for s in range(1, tpn):
        qcopies[s - 1].wait_recv()
        square = square + sqrecv[lax.rem(tp + tpn - s, tpn)]
    scale = lax.rsqrt(square[:, :1] / width + EPS)
    moe[span(me, seq), mine] = (total * scale * gain[:, mine]).astype(BF16)

    def block(e, t):
        return moe.at[span(e, seq), span(t, cols)]

    copies = []
    ecopies = [None]
    for s in range(1, n):
        copy = send(block(me, tp), block(me, tp), esems, s, {"ep": lax.rem(me + s, n)})
        copy.start()
        ecopies.append(copy)
    ycopies, ccopies = {}, {}
    for s in range(n):
        e = lax.rem(me + n - s, n)
        if s:
            ecopies[s].wait_recv()
        for q in range(1, sides):
            peer = lax.rem(side + q, sides) * CORES + core
            copy = send(block(e, tp), block(e, tp), ysems, s * sides + q, {"tp": peer})
            copy.start()
            ycopies[s, q] = copy
        copy = send(block(e, tp), block(e, tp), csems, s * sides, {"tp": twin})
        copy.start()
        ccopies[s, 0] = copy
    for s in range(n):
        e = lax.rem(me + n - s, n)
        for q in range(1, sides):
            ycopies[s, q].wait_recv()
            t = lax.rem(side + sides - q, sides) * CORES + core
            copy = send(block(e, t), block(e, t), csems, s * sides + q, {"tp": twin})
            copy.start()
            ccopies[s, q] = copy
    for copy in ccopies.values():
        copy.wait()
    for copy in list(ycopies.values()) + ecopies[1:] + hcopies + qcopies:
        copy.wait_send()


def reduce_kernel(
    n, tpn, part, shared, resid, out, crecv, ysend, yrecv, esend, erecv, *sems
):
    csems, ysems, esems = [(sems[2 * i], sems[2 * i + 1]) for i in range(3)]
    me = lax.axis_index("ep")
    tp = lax.axis_index("tp")
    seq, cols = resid.shape
    side, core = lax.div(tp, CORES), lax.rem(tp, CORES)
    sides = tpn // CORES
    twin = side * CORES + (CORES - 1 - core)
    greet(n, tpn, me, tp)
    order = list(range(1, n)) + [n, 0]

    def block(s, t):
        if s == n:
            return shared.at[:, span(t, cols)]
        return part.at[span(lax.rem(me + s, n), seq), span(t, cols)]

    turns = list(range(1, sides)) + [0]
    ccopies, ycopies, ecopies = {}, {}, {}
    for s in order:
        for q in turns:
            t = lax.rem(side + q, sides) * CORES + (CORES - 1 - core)
            i = s * sides + q
            copy = send(block(s, t), crecv.at[i], csems, i, {"tp": twin})
            copy.start()
            ccopies[s, q] = copy
    kept = {}
    for s in order:
        for q in turns[:-1]:
            peer = lax.rem(side + q, sides) * CORES + core
            i = s * sides + q
            ccopies[s, q].wait_recv()
            both = block(s, peer)[...].astype(F32) + crecv[i].astype(F32)
            ysend[i] = both.astype(BF16)
            copy = send(ysend.at[i], yrecv.at[i], ysems, i, {"tp": peer})
            copy.start()
            ycopies[s, q] = copy
    last = None
    for s in order:
        i = s * sides
        ccopies[s, 0].wait_recv()
        both = block(s, tp)[...].astype(F32) + crecv[i].astype(F32)
        for q in turns[:-1]:
            ycopies[s, q].wait_recv()
            both = both + yrecv[i + q].astype(F32)
        if 0 < s < n:
            esend[s] = both.astype(BF16)
            copy = send(esend.at[s], erecv.at[s], esems, s, {"ep": lax.rem(me + s, n)})
            copy.start()
            ecopies[s] = copy
        else:
            last = both if last is None else last + both
    last = last + resid[...]
    for s in range(1, n):
        ecopies[s].wait_recv()
        last = last + erecv[s].astype(F32)
    out[...] = last.astype(BF16)
    for group in (ccopies, ycopies, ecopies):
        for copy in group.values():
            copy.wait_send()


def pairs(counts):
    return [pltpu.SemaphoreType.DMA((c,)) for c in counts for _ in range(2)]


def call(kernel, outs, ins, spaces, out_spaces, scratch, ident):
    return pl.pallas_call(
        kernel,
        out_shape=outs,
        in_specs=[pl.BlockSpec(memory_space=s) for s in spaces],
        out_specs=[pl.BlockSpec(memory_space=s) for s in out_spaces],
        scratch_shapes=scratch,
        compiler_params=pltpu.CompilerParams(
            collective_id=ident, has_side_effects=True, vmem_limit_bytes=VMEM_BYTES
        ),
    )(*ins)


def local(
    tokens,
    state,
    norm_gain,
    w_query,
    w_forget,
    w_input,
    w_outgate,
    lower_bound,
    head_gain,
    w_output,
    ffn_gain,
    route_ids,
    route_weight,
    expert_gate,
    expert_up,
    expert_down,
    shared_gate,
    shared_up,
    shared_down,
    dense_gate,
    dense_up,
    dense_down,
    dense_mix,
):
    n = lax.axis_size("ep")
    tpn = lax.axis_size("tp")
    seq, width = tokens.shape
    depth, mix_local = w_query.shape
    heads_local = state.shape[1]
    head_dim = state.shape[2]
    cols = width // tpn
    exp_local = expert_gate.shape[0]
    experts = exp_local * n
    slots = -(-experts // LANES) * LANES
    sds = jax.ShapeDtypeStruct
    VM, ANY = pltpu.VMEM, pl.ANY

    route = jnp.sum(
        jnp.where(
            route_ids[:, :, None] == jnp.arange(slots, dtype=jnp.int32)[None, None, :],
            route_weight[:, :, None],
            jnp.float32(0.0),
        ),
        axis=1,
    )
    mix = jnp.broadcast_to(jax.nn.sigmoid(dense_mix)[None, :], (8, cols))
    dense_cols = dense_gate.shape[1] // tpn
    move = dense_cols % LANES == 0
    ins = [tokens, norm_gain[None, :], route, mix, w_query, w_forget, w_input, w_outgate]
    outs = [
        sds((seq, 4 * mix_local), BF16),
        sds((n, seq, slots), F32),
        sds((tpn, 8, cols), F32),
    ]
    scratch = [
        VM((n, seq, depth), BF16),
        VM((n, seq, depth), BF16),
        VM((n, seq, 4 * mix_local), BF16),
        VM((n, seq, 4 * mix_local), BF16),
    ] + pairs([n, n, n, tpn])
    spaces, out_spaces = [VM] * len(ins), [VM] * len(outs)
    if move:
        ins += [dense_gate, dense_up, dense_down]
        outs += [sds((width, dense_cols), BF16)] * 2 + [sds((dense_cols, width), BF16)]
        spaces += [ANY] * 3
        out_spaces += [ANY] * 3
        scratch += pairs([3 * tpn]) + [pltpu.SemaphoreType.DMA((3,))]
    res = call(
        functools.partial(front_kernel, n, tpn, move), outs, ins, spaces, out_spaces, scratch, 0
    )
    projected, route_all, mix_all = res[:3]
    if move:
        gate_w, up_w, down_w = res[3:]
    else:
        gate_w, up_w = [
            lax.all_to_all(w, "tp", split_axis=1, concat_axis=0, tiled=True)
            for w in (dense_gate, dense_up)
        ]
        down_w = lax.all_to_all(dense_down, "tp", split_axis=0, concat_axis=1, tiled=True)

    query, forget_pre, values, out_gate = jnp.split(projected.astype(F32), 4, axis=1)
    shape = (seq, heads_local, head_dim)
    forget_sig = jax.nn.sigmoid(forget_pre)
    decay = (lower_bound + (1.0 - lower_bound) * forget_sig).reshape(shape)
    keygate = ((1.0 - lower_bound) * (1.0 - forget_sig)).reshape(shape)
    new_state = decay[..., None] * state + keygate[..., None] * values.reshape(shape)[:, :, None, :]
    readout = jnp.einsum(
        "bhk,bhkv->bhv", query.reshape(shape), new_state, precision=lax.Precision.HIGHEST
    )
    readout = readout * lax.rsqrt(jnp.mean(readout * readout, axis=-1, keepdims=True) + EPS)
    head_out = (readout.reshape(seq, mix_local) * head_gain * jax.nn.silu(out_gate)).astype(BF16)

    sides = tpn // CORES
    resid, moe_in = call(
        functools.partial(gather_kernel, n, tpn),
        [sds((seq, cols), F32), sds((n * seq, width), BF16)],
        [tokens, ffn_gain[None, :], head_out, w_output],
        [VM] * 4,
        [VM] * 2,
        [
            VM((tpn, seq, cols), BF16),
            VM((tpn, seq, cols), BF16),
            VM((seq, LANES), F32),
            VM((tpn, seq, LANES), F32),
        ]
        + pairs([tpn, tpn, n, n * sides, n * sides]),
        1,
    )

    ep_index = lax.axis_index("ep")
    own = lax.dynamic_slice_in_dim(moe_in, ep_index * seq, seq, 0)
    shared_hidden = (
        jax.nn.silu(jnp.dot(own, shared_gate, preferred_element_type=F32))
        * jnp.dot(own, shared_up, preferred_element_type=F32)
    ).astype(BF16)
    shared_part = jnp.dot(shared_hidden, shared_down, preferred_element_type=F32).astype(BF16)

    route_rows = lax.dynamic_slice_in_dim(
        route_all.reshape(n * seq, slots), ep_index * exp_local, exp_local, 1
    )
    part = jnp.zeros((n * seq, width), F32)
    for e in range(exp_local):
        gate_pre = jnp.dot(moe_in, expert_gate[e], preferred_element_type=F32)
        up_pre = jnp.dot(moe_in, expert_up[e], preferred_element_type=F32)
        hidden = (jax.nn.silu(gate_pre) * up_pre * route_rows[:, e : e + 1]).astype(BF16)
        part = part + jnp.dot(hidden, expert_down[e], preferred_element_type=F32)
    dense_hidden = (
        jax.nn.silu(jnp.dot(moe_in, gate_w, preferred_element_type=F32))
        * jnp.dot(moe_in, up_w, preferred_element_type=F32)
    ).astype(BF16)
    mix_row = mix_all[:, 0, :].reshape(1, width)
    part = part + mix_row * jnp.dot(dense_hidden, down_w, preferred_element_type=F32)
    blocks = (n + 1) * sides
    (mixed,) = call(
        functools.partial(reduce_kernel, n, tpn),
        [sds((seq, cols), BF16)],
        [part.astype(BF16), shared_part, resid],
        [VM] * 3,
        [VM],
        [VM((blocks, seq, cols), BF16)] * 3 + [VM((n, seq, cols), BF16)] * 2
        + pairs([blocks, blocks, n]),
        2,
    )
    return (mixed, new_state)


def solution(mesh):
    placed = (
        P("ep", None),
        P("ep", "tp", None, None),
        P(),
        P("ep", "tp"),
        P("ep", "tp"),
        P("ep", "tp"),
        P("ep", "tp"),
        P("tp"),
        P("tp"),
        P("tp", None),
        P(),
        P("ep", None),
        P("ep", None),
        P("ep", None, "tp"),
        P("ep", None, "tp"),
        P("ep", "tp", None),
        P(None, "tp"),
        P(None, "tp"),
        P("tp", None),
        P("tp", "ep"),
        P("tp", "ep"),
        P("ep", "tp"),
        P("tp"),
    )
    return jax.shard_map(
        local,
        mesh=mesh,
        in_specs=placed,
        out_specs=(P("ep", "tp"), P("ep", "tp", None, None)),
        check_vma=False,
    )
```

profile of v0, /device:TPU:0, one launch (start us, length us, event | category | flops | bytes accessed | tf_op | source)
XLA Modules:
  0.0 140.2 jit_solution(10680880252173510638)
XLA Ops:
  0.6 0.0 copy-start
  0.6 1.5 %select_reduce_fusion.refs_2_ = f32[48,128]{1,0:T(8,128)} fusion(f32[48,4]{0,1:T(4,128)} %param.35, s32[48,4]{0,1:T(4,128)} %param.34), kind=kLoop, calls=%fused_computation.54 | loop fusion | flops 67584 | bytes 26112 | tf_op jit(solution)/shard_map/reduce_sum | solution.py:346
  2.2 0.7 add_divide_fusion
  2.8 0.6 broadcast_in_dim.36.refs_3_
  3.5 0.0 copy-start.4
  3.5 45.3 %shard_map.230 = (bf16[48,1024]{1,0:T(8,128)(2,1)}, f32[8,48,128]{2,1,0:T(8,128)}, f32[4,8,512]{2,1,0:T(8,128)}, bf16[2048,256]{1,0:T(8,128)(2,1)}, bf16[2048,25...) custom-call(bf16[48,2048]{1,0:T(8,128)(2,1)} %tokens.1, f32[1,2048]{1,0:T(1,128)} %bitcast.52, ...), custom_call_target="tpu_custom_call" | custom-call | tf_op jit(solution)/shard_map/pallas_call | solution.py:296
  48.8 0.7 split.12
  49.5 0.7 split.17
  50.3 0.0 copy-done.4
  50.3 0.9 convert_element_type.24
  51.3 7.1 %multiply_add_fusion = f32[48,2,128,128]{3,2,1,0:T(8,128)S(1)} fusion(f32[48,2,128,128]{3,2,1,0:T(8,128)} %param.24, f32[48,2,128]{2,1,0:T(2,128)S(1)} %mul.136, f32[48,2,128]{2,1,0:T(2,128)S(1)} %mul.134, f32[48,2,128]{2,1,0:T(2,128)S(1)} %mul.130), kind=kLoop, calls=%fused_computation | loop fusion | flops 4718592 | bytes 12730368 | tf_op jit(solution)/shard_map/add | solution.py:394
  58.5 0.0 copy-start.1
  58.5 0.0 copy-start.5
  58.5 3.0 %fusion.68 = f32[48,2,1,128]{3,2,1,0:T(1,128)S(1)} fusion(bf16[48,2,128,1]{2,3,1,0:T(2,128)(2,1)S(1)} %reshape.37, f32[48,2,128,128]{3,2,1,0:T(8,128)S(1)} %multiply_add_fusion), kind=kOutput, calls=%fused_computation.82 | convolution fusion | flops 18874368 | bytes 6365184 | tf_op jit(solution)/shard_map/bhk,bhkv->bhv/dot_general | solution.py:395
  61.4 0.0 copy-done.1
  61.4 0.1 multiply_reduce_fusion
  61.6 0.1 broadcast_multiply_fusion
  61.7 0.0 copy-done.5
  61.7 0.6 fusion.51.head
  62.4 26.5 %shard_map.231 = (f32[48,512]{1,0:T(8,128)}, bf16[384,2048]{1,0:T(8,128)(2,1)}) custom-call(bf16[48,2048]{1,0:T(8,128)(2,1)} %tokens.1, f32[1,2048]{1,0:T(1,128)} %bitcast.53, bf16[48,256]{1,0:T(8,128)(2,1)} %fusion.51.head, bf16[256,2048]{1,0:T(8,128)(2,1)} %wout.1), custom_call_target="tpu_custom_call" | custom-call | tf_op jit(solution)/shard_map/pallas_call | solution.py:296
  88.8 0.0 copy-start.3
  88.9 0.0 copy-start.2
  88.9 2.4 %fusion.16 = f32[384,256]{1,0:T(8,128)S(1)} fusion(bf16[384,2048]{1,0:T(8,128)(2,1)} %get-tuple-element.11, bf16[2,2048,256]{2,1,0:T(8,128)(2,1)} %param.36), kind=kOutput, calls=%fused_computation.21 | convolution fusion | flops 402653184 | bytes 3014656 | tf_op jit(solution)/shard_map/dot_general | solution.py:431
  91.3 0.0 copy-done.3
  91.3 0.3 dynamic-slice_reduce_fusion
  91.6 0.0 copy-done.2
  91.6 5.0 %fusion.5 = f32[384,2048]{1,0:T(8,128)} fusion(bf16[384,2048]{1,0:T(8,128)(2,1)S(1)} %copy-done.2, bf16[2,256,2048]{2,1,0:T(8,128)(2,1)} %param.38, bf16[2,2048,256]{2,1,0:T(8,128)(2,1)} %param.37, f32[384,256]{1,0:T(8,128)S(1)} %fusion.16, f32[384]{0:T(512)S(1)} %get-tuple-element.19), kind=kOutput, calls=%fused_computation.11 | convolution fusion | flops 805994496 | bytes 7210496 | tf_op jit(solution)/shard_map/dot_general | solution.py:434
  96.6 1.8 %fusion.11 = f32[384,256]{1,0:T(8,128)S(1)} fusion(bf16[384,2048]{1,0:T(8,128)(2,1)S(1)} %copy-done.2, bf16[2,2048,256]{2,1,0:T(8,128)(2,1)} %param.36), kind=kOutput, calls=%fused_computation.17 | convolution fusion | flops 402653184 | bytes 3014656 | tf_op jit(solution)/shard_map/dot_general | solution.py:431
  98.4 5.0 %fusion.6 = f32[384,2048]{1,0:T(8,128)} fusion(bf16[384,2048]{1,0:T(8,128)(2,1)S(1)} %copy-done.2, bf16[2,256,2048]{2,1,0:T(8,128)(2,1)} %param.38, bf16[2,2048,256]{2,1,0:T(8,128)(2,1)} %param.37, f32[384,256]{1,0:T(8,128)S(1)} %fusion.11, f32[384]{0:T(512)S(1)} %get-tuple-element.18), kind=kOutput, calls=%fused_computation.12 | convolution fusion | flops 805994496 | bytes 7210496 | tf_op jit(solution)/shard_map/dot_general | solution.py:434
  103.5 0.8 slice.35
  104.3 1.8 %fusion.69 = f32[384,256]{1,0:T(8,128)S(1)} fusion(bf16[384,2048]{1,0:T(8,128)(2,1)S(1)} %copy-done.2, bf16[2048,256]{1,0:T(8,128)(2,1)} %get-tuple-element.14), kind=kOutput, calls=%fused_computation.83 | convolution fusion | flops 402653184 | bytes 3014656 | tf_op jit(solution)/shard_map/dot_general | solution.py:436
  106.1 6.4 %add_convert_fusion.part = bf16[384,2048]{1,0:T(8,128)(2,1)} fusion(f32[384,2048]{1,0:T(8,128)} %fusion.5, f32[384,2048]{1,0:T(8,128)} %fusion.6, bf16[256,2048]{1,0:T(8,128)(2,1)} %get-tuple-element.16, f32[2048]{0:T(1024)S(1)} %bitcast.51, bf16[384,2048]{1,0:T(8,128)(2,1)S(1)} %copy-done.2, bf16[2048,256]{1,0:T(8,128)(2,1)} %get-tuple-element.15, ...), kind=kOutput, calls=%fused_computation.1 | convolution fusion | flops 809041920 | bytes 11935744 | tf_op jit(solution)/shard_map/dot_general | solution.py:440
  112.5 1.5 %fusion.48 = f32[48,256]{1,0:T(8,128)S(1)} fusion(bf16[2048,256]{1,0:T(8,128)(2,1)} %param.39, bf16[384,2048]{1,0:T(8,128)(2,1)S(1)} %copy-done.2, s32[]{:T(128)S(6)} %select_n.12), kind=kOutput, calls=%fused_computation.52 | convolution fusion | flops 50331648 | bytes 1294340 | tf_op jit(solution)/shard_map/dot_general | solution.py:421
  114.0 0.0 copy-done
  114.1 2.7 %convolution_convert_fusion.shared = bf16[48,2048]{1,0:T(8,128)(2,1)} fusion(bf16[256,2048]{1,0:T(8,128)(2,1)S(1)} %copy-done, bf16[2048,256]{1,0:T(8,128)(2,1)} %param.40, bf16[384,2048]{1,0:T(8,128)(2,1)S(1)} %copy-done.2, s32[]{:T(128)S(6)} %select_n.12, f32[48,256]{1,0:T(8,128)S(1)} %fusion.48), kind=kOutput, calls=%fused_computation.2 | convolution fusion | flops 100835328 | bytes 2539524 | tf_op jit(solution)/shard_map/dot_general | solution.py:424
  116.7 22.1 %shard_map.232 = bf16[48,512]{1,0:T(8,128)(2,1)} custom-call(bf16[384,2048]{1,0:T(8,128)(2,1)} %add_convert_fusion.part, bf16[48,2048]{1,0:T(8,128)(2,1)} %convolution_convert_fusion.shared, f32[48,512]{1,0:T(8,128)} %get-tuple-element.17.resid), custom_call_target="tpu_custom_call" | custom-call | tf_op jit(solution)/shard_map/pallas_call | solution.py:296
  138.8 1.4 %copy.47 = bf16[48,512]{1,0:T(8,128)(2,1)} copy(bf16[48,512]{1,0:T(8,128)(2,1)} %shard_map.232) | data formatting | bytes 98304
  (7 shorter events, 0.1 us)
Async XLA Ops:
  0.6 113.4 %copy-start = (bf16[256,2048]{1,0:T(8,128)(2,1)S(1)}, bf16[256,2048]{1,0:T(8,128)(2,1)}, u32[]{:S(2)}) copy-start(bf16[256,2048]{1,0:T(8,128)(2,1)} %param.41) | copy-start | bytes 3145732
  3.5 46.8 %copy-start.4 = (f32[256]{0:T(256)S(1)}, f32[256]{0:T(256)}, u32[]{:S(2)}) copy-start(f32[256]{0:T(256)} %param.30) | copy-start | bytes 3076
  58.5 3.0 %copy-start.1 = (f32[48,2,128,128]{3,2,1,0:T(8,128)}, f32[48,2,128,128]{3,2,1,0:T(8,128)S(1)}, u32[]{:S(2)}) copy-start(f32[48,2,128,128]{3,2,1,0:T(8,128)S(1)} %multiply_add_fusion) | copy-start | bytes 18874372
  58.5 3.3 %copy-start.5 = (f32[256]{0:T(256)S(1)}, f32[256]{0:T(256)}, u32[]{:S(2)}) copy-start(f32[256]{0:T(256)} %param.31) | copy-start | bytes 3076
  88.8 2.4 %copy-start.3 = (f32[8,48,128]{2,1,0:T(8,128)S(1)}, f32[8,48,128]{2,1,0:T(8,128)}, u32[]{:S(2)}) copy-start(f32[8,48,128]{2,1,0:T(8,128)} %get-tuple-element.12) | copy-start | bytes 589828
  88.9 2.7 %copy-start.2 = (bf16[384,2048]{1,0:T(8,128)(2,1)S(1)}, bf16[384,2048]{1,0:T(8,128)(2,1)}, u32[]{:S(2)}) copy-start(bf16[384,2048]{1,0:T(8,128)(2,1)} %get-tuple-element.11) | copy-start | bytes 4718596
where the time goes:
time: 141 us; the launch traced here: 140 us
  Pallas kernels  93.9 us (67%)
  matrix products  29.6 us (21%)
  other arithmetic  11.1 us (8%)
  local copies, waits for them, and re-layouts  4.81 us (3%)
    pallas_call x3, Pallas kernels, call(): pl.pallas_call(kernel, out_shape=outs, in_specs=[pl.BlockSpec(memory_spac...  93.9 us
    dot_general x2, matrix products, local(): part = part + jnp.dot(hidden, expert_down[e], preferred_element_type=F32)  10 us
    add x1, other arithmetic, local(): decay[..., None] * state  7.12 us
    dot_general x1, matrix products, local(): jnp.dot(dense_hidden, down_w, preferred_element_type=F32)  6.42 us
    dot_general x2, matrix products, local(): gate_pre = jnp.dot(moe_in, expert_gate[e], preferred_element_type=F32)  4.2 us
    dot_general x1, matrix products, local(): jnp.einsum('bhk,bhkv->bhv', query.reshape(shape), new_state, precision=la...  2.96 us

commit v1 on v0

v1 whole, which is shorter than its diff:
```python
import functools
import types

import jax
import jax.numpy as jnp
from jax import lax
from jax.experimental import pallas as pl
from jax.experimental.pallas import tpu as pltpu
from jax.sharding import PartitionSpec as P

EPS = 1e-06
LANES = 128
CORES = 2
ROWS = 8
F32 = jnp.float32
BF16 = jnp.bfloat16
VMEM_BYTES = 60 * 1024 * 1024
(
    WEIGHT,
    NORMED,
    MOVE,
    ROUTE,
    MIX,
    PROJ,
    HEAD,
    GATHER_Z,
    GATHER_A,
    GATHER_B,
    GATHER_C,
    SQUARE,
    SCALE,
    SUM_C,
    SUM_A,
    SUM_B,
    SUM_Z,
) = range(17)


def span(index, size):
    if isinstance(index, int):
        return pl.ds(index * size, size)
    return pl.ds(pl.multiple_of(index * size, size), size)


def ceil_to(value, step):
    return -(-value // step) * step


def silu(v):
    return v * jax.nn.sigmoid(v)


def layer_kernel(n, tpn, move, names, *refs):
    sems = refs[len(names) :]
    r = types.SimpleNamespace(**dict(zip(names, refs)))
    me, tp = lax.axis_index("ep"), lax.axis_index("tp")
    sides = tpn // CORES
    xs = sides
    zs = n // xs
    z, x = lax.div(me, xs), lax.rem(me, xs)
    y, c = lax.div(tp, CORES), lax.rem(tp, CORES)
    twin_core = CORES - 1 - c
    seq, width = r.tokens.shape
    cols = width // tpn
    depth, mixw = r.wq.shape
    exp_local, _, ff = r.eg.shape
    sff = r.sg.shape[1]
    dff = r.dgv.shape[2]
    heads, hd = r.state.shape[1:3]
    wrap = xs * depth
    lanes = r.scs.shape[1]
    half = sides * cols

    def pick(first, second):
        return first * (1 - c) + second * c

    def device(zz, xx, yy, cc):
        return {"ep": zz * xs + xx, "tp": yy * CORES + cc}

    waiting = []

    def send(src, dst, kind, slot, peer):
        copy = pltpu.make_async_remote_copy(
            src_ref=src,
            dst_ref=dst,
            send_sem=sems[2 * kind].at[slot],
            recv_sem=sems[2 * kind + 1].at[slot],
            device_id=peer,
            device_id_type=pl.DeviceIdType.MESH,
        )
        copy.start()
        waiting.append(copy)
        return copy

    used = [0]

    def fetch(src, dst):
        copy = pltpu.make_async_copy(src, dst, r.local.at[used[0]])
        used[0] += 1
        copy.start()
        return copy

    got = types.SimpleNamespace()
    got.tokens = fetch(r.tokens, r.tokens_v)
    got.gain1 = fetch(r.gain1, r.gain1_v)
    order = (r.wf, r.wq, r.wi, r.wo)
    got.w = [fetch(w, r.wbuf.at[i, span(x, depth), :]) for i, w in enumerate(order)]
    got.lb = fetch(r.lb, r.lb_v)
    got.hg = fetch(r.hg, r.hg_v)
    got.mix = fetch(r.mix, r.mix_v)
    got.ids = fetch(r.ids, r.ids_v)
    got.weights = fetch(r.weights, r.weights_v)
    groups = seq // ROWS
    states = [
        fetch(r.state.at[pl.ds(g * ROWS, ROWS)], r.st.at[pl.ds(g * ROWS, ROWS)])
        for g in range(groups)
    ]
    got.wout = fetch(r.wout, r.wout_v)
    got.gain2 = fetch(r.gain2, r.gain2_v)

    barrier = pltpu.get_barrier_semaphore()
    for s in range(1, tpn):
        pl.semaphore_signal(
            barrier,
            inc=1,
            device_id={"tp": lax.rem(tp + s, tpn)},
            device_id_type=pl.DeviceIdType.MESH,
        )
    for s in range(1, n):
        pl.semaphore_signal(
            barrier,
            inc=1,
            device_id={"ep": lax.rem(me + s, n)},
            device_id_type=pl.DeviceIdType.MESH,
        )
    got.tokens.wait()
    got.gain1.wait()
    t32 = r.tokens_v[...].astype(F32)
    normed = (
        t32 * lax.rsqrt(jnp.mean(t32 * t32, axis=-1, keepdims=True) + EPS) * r.gain1_v[...]
    ).astype(BF16)
    for d in range(zs):
        r.nsend[d * seq : (d + 1) * seq, :] = normed[:, d * wrap : (d + 1) * wrap]
    r.ncol[span(z, seq), :] = r.nsend[span(z, seq), :]
    pl.semaphore_wait(barrier, n - 1 + tpn - 1)

    arrived = {}
    for i, w in enumerate(order):
        for s in range(1, xs):
            arrived[WEIGHT, i, s] = send(
                w,
                r.wbuf.at[i, span(x, depth), :],
                WEIGHT,
                i * xs + s,
                device(z, lax.rem(x + s, xs), y, c),
            )
    for s in range(1, zs):
        zz = lax.rem(z + s, zs)
        arrived[NORMED, s] = send(
            r.nsend.at[span(zz, seq)],
            r.ncol.at[span(z, seq)],
            NORMED,
            s,
            device(zz, x, y, c),
        )
    if move:
        got.dgv = []
        for i, (src, dst) in enumerate(((r.dgate, r.dgv), (r.dup, r.duv))):
            rows = src.shape[0]
            for s in range(1, tpn):
                peer = lax.rem(tp + s, tpn)
                arrived[MOVE, i, s] = send(
                    src.at[:, span(peer, dff)],
                    dst.at[c, span(y, rows), :],
                    MOVE,
                    i * tpn + s,
                    {"tp": peer},
                )
            got.dgv.append(fetch(src.at[:, span(tp, dff)], dst.at[c, span(y, rows), :]))

    got.ids.wait()
    got.weights.wait()
    got.mix.wait()
    eye = lax.broadcasted_iota(jnp.int32, (seq, lanes), 0) == lax.broadcasted_iota(
        jnp.int32, (seq, lanes), 1
    )
    ids, weights = r.ids_v[...], r.weights_v[...]
    rrows = r.rsend.shape[1]

    def to_row(col):
        return jnp.sum(jnp.where(eye, col, 0.0), axis=0, keepdims=True)

    def to_col(row):
        return jnp.sum(jnp.where(eye, row, 0.0), axis=1, keepdims=True)

    for d in range(n):
        r.rsend[d] = jnp.zeros((rrows, lanes), F32)
        for i in range(exp_local):
            r.rsend[d, i : i + 1, :seq] = jnp.sum(
                jnp.where(ids == d * exp_local + i, weights, 0.0), axis=0, keepdims=True
            )
    r.rrecv[me] = r.rsend[me]
    for s in range(1, n):
        peer = lax.rem(me + s, n)
        arrived[ROUTE, s] = send(
            r.rsend.at[peer], r.rrecv.at[me], ROUTE, s, {"ep": peer}
        )
    r.mixs[...] = jnp.broadcast_to(jax.nn.sigmoid(r.mix_v[...]), (ROWS, cols))
    r.mixr[tp] = r.mixs[...]
    for s in range(1, tpn):
        arrived[MIX, s] = send(
            r.mixs, r.mixr.at[tp], MIX, s, {"tp": lax.rem(tp + s, tpn)}
        )

    def fetch_rows(src, dst):
        return [
            fetch(src.at[span(t, cols), :], dst(t % CORES).at[span(t // CORES, cols), :])
            for t in range(tpn)
        ]

    got.sgv = fetch_rows(r.sg, lambda k: r.sgv.at[k]) + fetch_rows(r.su, lambda k: r.suv.at[k])
    got.sdv = [fetch(r.sd, r.sdv)]
    got.egv = []
    for e in range(exp_local):
        got.egv += fetch_rows(r.eg.at[e], lambda k: r.egv.at[k, e])
        got.egv += fetch_rows(r.eu.at[e], lambda k: r.euv.at[k, e])
    got.edv = [fetch(r.ed.at[e], r.edv.at[span(e, ff), :]) for e in range(exp_local)]
    if move:
        got.ddv = [fetch(r.ddown.at[span(tp, dff), :], r.ddv.at[tp])]
    else:
        got.dgv = fetch_rows(r.gatew, lambda k: r.dgv.at[k])
        got.dgv += fetch_rows(r.upw, lambda k: r.duv.at[k])
        got.ddv = [fetch(r.downw.at[:, span(t, cols)], r.ddv.at[t]) for t in range(tpn)]

    for s in range(1, zs):
        arrived[NORMED, s].wait_recv()
    for i in range(len(order)):
        got.w[i].wait()
        for s in range(1, xs):
            arrived[WEIGHT, i, s].wait_recv()
        r.psend[i] = jnp.dot(
            r.ncol[...], r.wbuf[i], preferred_element_type=F32
        ).astype(BF16)
        for s in range(1, zs):
            zz = lax.rem(z + s, zs)
            arrived[PROJ, i, s] = send(
                r.psend.at[i, span(zz, seq)],
                r.precv.at[i, span(z, seq)],
                PROJ,
                i * zs + s,
                device(zz, x, y, c),
            )

    def projected(i):
        total = r.psend[i, span(z, seq), :].astype(F32)
        for s in range(1, zs):
            arrived[PROJ, i, s].wait_recv()
            total = total + r.precv[i, span(lax.rem(z + zs - s, zs), seq), :].astype(F32)
        return total.astype(BF16).astype(F32)

    padded = ceil_to(seq, LANES)

    def turn(value, dst):
        if padded > seq:
            value = jnp.concatenate([value, jnp.zeros((padded - seq, mixw), F32)], axis=0)
        value = value.T
        for g in range(groups):
            dst[g] = value[:, g * ROWS : (g + 1) * ROWS]

    got.lb.wait()
    got.hg.wait()
    lb = r.lb_v[...]
    turn(lb + (1.0 - lb) * jax.nn.sigmoid(projected(0)), r.dturn)
    turn(projected(1), r.qturn)
    r.vals[...] = projected(2)
    for copy in states:
        copy.wait()

    def group(g, carry):
        dg, qg = r.dturn[g], r.qturn[g]
        vg = r.vals[span(g, ROWS), :]
        rows = []
        for b in range(ROWS):
            parts = []
            for h in range(heads):
                at = slice(h * hd, (h + 1) * hd)
                vrow = vg[b : b + 1, at]
                new = vrow + dg[at, b : b + 1] * (r.st[g * ROWS + b, h] - vrow)
                r.st[g * ROWS + b, h] = new
                parts.append(jnp.sum(qg[at, b : b + 1] * new, axis=0, keepdims=True))
            rows.append(jnp.concatenate(parts, axis=1))
        r.read[span(g, ROWS), :] = jnp.concatenate(rows, axis=0)
        pltpu.make_async_copy(
            r.st.at[span(g, ROWS)], r.new_state.at[span(g, ROWS)], r.stout.at[g]
        ).start()
        return carry

    lax.fori_loop(0, groups, group, 0)
    read = r.read[...]
    read = jnp.concatenate(
        [
            part * lax.rsqrt(jnp.mean(part * part, axis=-1, keepdims=True) + EPS)
            for part in [read[:, h * hd : (h + 1) * hd] for h in range(heads)]
        ],
        axis=1,
    )
    head = (read * r.hg_v[...] * silu(projected(3))).astype(BF16)

    got.wout.wait()
    got.gain2.wait()
    for t in range(tpn):
        r.hsend[t] = jnp.dot(
            head, r.wout_v[:, t * cols : (t + 1) * cols], preferred_element_type=F32
        ).astype(BF16)
    for s in range(1, tpn):
        peer = lax.rem(tp + s, tpn)
        arrived[HEAD, s] = send(r.hsend.at[peer], r.hrecv.at[tp], HEAD, s, {"tp": peer})
    mine = span(tp, cols)
    total = r.tokens_v[:, mine].astype(F32) + r.hsend[tp].astype(F32)
    for s in range(1, tpn):
        arrived[HEAD, s].wait_recv()
        total = total + r.hrecv[lax.rem(tp + tpn - s, tpn)].astype(F32)
    r.resid[...] = total

    def block(zz, xx, yy, cc):
        return r.rows.at[cc, span(zz * xs + xx, seq), span(yy, cols)]

    r.rows[c, span(me, seq), span(y, cols)] = (total * r.gain2_v[:, mine]).astype(BF16)
    own = block(z, x, y, c)
    for s in range(1, zs):
        arrived[GATHER_Z, s] = send(own, own, GATHER_Z, s, device(lax.rem(z + s, zs), x, y, c))

    def plane(s, a, b):
        zz = lax.rem(z + zs - s, zs)
        xx = lax.rem(x + xs - pick(a, b), xs)
        yy = lax.rem(y + sides - pick(b, a), sides)
        return block(zz, xx, yy, c)

    def forward_first(s):
        ref = plane(s, 0, 0)
        for q in range(1, sides):
            peer = device(z, lax.rem(x + pick(q, 0), xs), lax.rem(y + pick(0, q), sides), c)
            arrived[GATHER_A, s, q] = send(ref, ref, GATHER_A, s * sides + q, peer)

    def forward_second(s, a):
        ref = plane(s, a, 0)
        for q in range(1, sides):
            peer = device(z, lax.rem(x + pick(0, q), xs), lax.rem(y + pick(q, 0), sides), c)
            arrived[GATHER_B, s, a, q] = send(ref, ref, GATHER_B, (s * sides + a) * sides + q, peer)

    def forward_twin(s, a, b):
        ref = plane(s, a, b)
        arrived[GATHER_C, s, a, b] = send(
            ref, ref, GATHER_C, (s * sides + a) * sides + b, device(z, x, y, twin_core)
        )

    forward_first(0)
    forward_second(0, 0)
    forward_twin(0, 0, 0)

    square = to_row(jnp.sum(total * total, axis=-1, keepdims=True))
    r.sqs[...] = jnp.broadcast_to(square, (ROWS, lanes))
    for s in range(1, tpn):
        arrived[SQUARE, s] = send(
            r.sqs, r.sqr.at[tp], SQUARE, s, {"tp": lax.rem(tp + s, tpn)}
        )
    for s in range(1, tpn):
        arrived[SQUARE, s].wait_recv()
        square = square + r.sqr[lax.rem(tp + tpn - s, tpn)][:1]
    scale = lax.rsqrt(square / width + EPS)
    r.scs[...] = jnp.broadcast_to(scale, (ROWS, lanes))
    r.scr[me] = r.scs[...]
    for s in range(1, n):
        arrived[SCALE, s] = send(r.scs, r.scr.at[me], SCALE, s, {"ep": lax.rem(me + s, n)})

    for s in range(zs):
        if s:
            arrived[GATHER_Z, s].wait_recv()
            forward_first(s)
            forward_second(s, 0)
            forward_twin(s, 0, 0)
        for a in range(1, sides):
            arrived[GATHER_A, s, a].wait_recv()
            forward_second(s, a)
            forward_twin(s, a, 0)
    if move:
        for s in range(1, tpn):
            peer = lax.rem(tp + s, tpn)
            arrived[MOVE, 2, s] = send(
                r.ddown.at[span(peer, dff), :],
                r.ddv.at[tp],
                MOVE,
                2 * tpn + s,
                {"tp": peer},
            )
    for s in range(zs):
        for a in range(sides):
            for b in range(1, sides):
                arrived[GATHER_B, s, a, b].wait_recv()
                forward_twin(s, a, b)

    pairs = [(r.egv, r.euv, e) for e in range(exp_local)] + [(r.dgv, r.duv, None)]

    def weight(ref, lead, plane_at):
        return ref[plane_at] if lead is None else ref[plane_at, lead]

    for copy in got.egv:
        copy.wait()
    for k, (gate, up, lead) in enumerate(pairs):
        if lead is None:
            for copy in got.dgv:
                copy.wait()
            if move:
                for i in range(2):
                    for s in range(1, tpn):
                        arrived[MOVE, i, s].wait_recv()
        acc = r.acc if lead is not None else r.dacc
        base = 2 * k if lead is not None else 0
        for j, ref in enumerate((gate, up)):
            acc[base + j] = jnp.dot(
                r.rows[c], weight(ref, lead, c), preferred_element_type=F32
            )

    for s in range(zs):
        for a in range(sides):
            for b in range(sides):
                arrived[GATHER_C, s, a, b].wait_recv()

    for copy in got.sgv + got.sdv:
        copy.wait()
    for s in range(1, n):
        arrived[SCALE, s].wait_recv()
        arrived[ROUTE, s].wait_recv()
    for s in range(1, tpn):
        arrived[MIX, s].wait_recv()
    pre = []
    for ref in (r.sgv, r.suv):
        pre.append(
            sum(
                jnp.dot(r.rows[k, span(me, seq), :], ref[k], preferred_element_type=F32)
                for k in range(CORES)
            )
        )
    own_scale = to_col(scale)
    shared_hidden = (silu(own_scale * pre[0]) * (own_scale * pre[1])).astype(BF16)
    for t in range(tpn):
        r.shared[t] = jnp.dot(
            shared_hidden, r.sdv[:, t * cols : (t + 1) * cols], preferred_element_type=F32
        )

    scales = jnp.concatenate([to_col(r.scr[e][:1]) for e in range(n)], axis=0)
    for k, (gate, up, lead) in enumerate(pairs):
        acc = r.acc if lead is not None else r.dacc
        base = 2 * k if lead is not None else 0
        both = [
            scales
            * (
                acc[base + j]
                + jnp.dot(
                    r.rows[twin_core],
                    weight(ref, lead, twin_core),
                    preferred_element_type=F32,
                )
            )
            for j, ref in enumerate((gate, up))
        ]
        hidden = silu(both[0]) * both[1]
        if lead is None:
            r.dhid[...] = hidden.astype(BF16)
        else:
            share = jnp.concatenate(
                [to_col(r.rrecv[e][lead : lead + 1]) for e in range(n)], axis=0
            )
            r.hid[:, k * ff : (k + 1) * ff] = (hidden * share).astype(BF16)
    for copy in got.edv + got.ddv:
        copy.wait()
    if move:
        for s in range(1, tpn):
            arrived[MOVE, 2, s].wait_recv()

    def partial(t):
        routed = jnp.dot(
            r.hid[...], r.edv[:, span(t, cols)], preferred_element_type=F32
        )
        dense = jnp.dot(r.dhid[...], r.ddv[t], preferred_element_type=F32)
        return routed + r.mixr[t][:1] * dense

    for q in [*range(1, sides), 0]:
        yy = lax.rem(y + q, sides)
        t = yy * CORES + twin_core
        r.part[q] = partial(t).astype(BF16)
        r.part[q, span(me, seq), :] = (
            r.part[q, span(me, seq), :].astype(F32) + r.shared[t]
        ).astype(BF16)
        arrived[SUM_C, q] = send(
            r.part.at[q], r.crecv.at[q], SUM_C, q, device(z, x, y, twin_core)
        )
    for q in [*range(1, sides), 0]:
        yy = lax.rem(y + q, sides)
        t = yy * CORES + c
        mypart = partial(t)
        arrived[SUM_C, q].wait_recv()
        r.both[yy] = (mypart + r.crecv[q].astype(F32)).astype(BF16)
        r.both[yy, span(me, seq), :] = (
            r.both[yy, span(me, seq), :].astype(F32) + r.shared[t]
        ).astype(BF16)
    zorder = [*range(1, zs), 0]
    rorder = [*range(1, sides), 0]

    def summed(si, q, j):
        zz = lax.rem(z + si, zs)
        xx = lax.rem(x + pick(j, q), xs)
        yy = lax.rem(y + pick(q, j), sides)
        return r.both.at[yy, span(zz * xs + xx, seq), :]

    for si in zorder:
        for j in rorder:
            for q in range(1, sides):
                slot = (si * sides + j) * sides + q
                peer = device(
                    z, lax.rem(x + pick(0, q), xs), lax.rem(y + pick(q, 0), sides), c
                )
                arrived[SUM_A, si, j, q] = send(
                    summed(si, q, j), r.arecv.at[slot], SUM_A, slot, peer
                )

    def second(si):
        for j in rorder:
            value = summed(si, 0, j)[...].astype(F32)
            for q in range(1, sides):
                arrived[SUM_A, si, j, q].wait_recv()
                value = value + r.arecv[(si * sides + j) * sides + q].astype(F32)
            if j == 0:
                r.keep[si] = value
                continue
            slot = si * sides + j
            r.bsend[slot] = value.astype(BF16)
            peer = device(z, lax.rem(x + pick(j, 0), xs), lax.rem(y + pick(0, j), sides), c)
            arrived[SUM_B, si, j] = send(r.bsend.at[slot], r.brecv.at[slot], SUM_B, slot, peer)

    def third(si):
        value = r.keep[si]
        for j in range(1, sides):
            arrived[SUM_B, si, j].wait_recv()
            value = value + r.brecv[si * sides + j].astype(F32)
        if si == 0:
            return value
        r.zsend[si] = value.astype(BF16)
        arrived[SUM_Z, si] = send(
            r.zsend.at[si],
            r.zrecv.at[si],
            SUM_Z,
            si,
            device(lax.rem(z + si, zs), x, y, c),
        )
        return None

    for k, si in enumerate(zorder):
        second(si)
        if k:
            third(zorder[k - 1])
    final = third(0) + r.resid[...]
    for s in range(1, zs):
        arrived[SUM_Z, s].wait_recv()
        final = final + r.zrecv[s].astype(F32)
    r.out[...] = final.astype(BF16)
    for copy in waiting:
        copy.wait_send()
    for g in range(groups):
        pltpu.make_async_copy(
            r.st.at[span(g, ROWS)], r.new_state.at[span(g, ROWS)], r.stout.at[g]
        ).wait()


def place_kernel(held, held_state, out, new_state, buf, st, sems):
    size = held_state.shape[0]
    parts = [pl.ds(g * ROWS, ROWS) for g in range(size // ROWS)]
    moves = [(held, buf, out)]
    moves += [(held_state.at[p], st.at[p], new_state.at[p]) for p in parts]
    first = [
        pltpu.make_async_copy(src, mid, sems.at[0, k]) for k, (src, mid, _) in enumerate(moves)
    ]
    last = [
        pltpu.make_async_copy(mid, dst, sems.at[1, k]) for k, (_, mid, dst) in enumerate(moves)
    ]
    for copy in first:
        copy.start()
    for copy, after in zip(first, last):
        copy.wait()
        after.start()
    for copy in last:
        copy.wait()


def local(
    tokens,
    state,
    norm_gain,
    w_query,
    w_forget,
    w_input,
    w_outgate,
    lower_bound,
    head_gain,
    w_output,
    ffn_gain,
    route_ids,
    route_weight,
    expert_gate,
    expert_up,
    expert_down,
    shared_gate,
    shared_up,
    shared_down,
    dense_gate,
    dense_up,
    dense_down,
    dense_mix,
):
    n = lax.axis_size("ep")
    tpn = lax.axis_size("tp")
    sides = tpn // CORES
    zs = n // sides
    seq, width = tokens.shape
    depth, mixw = w_query.shape
    heads, hd = state.shape[1:3]
    cols = width // tpn
    half = sides * cols
    exp_local, _, ff = expert_gate.shape
    sff = shared_gate.shape[1]
    dff = dense_gate.shape[1] // tpn
    lanes = ceil_to(seq, LANES)
    rrows = ceil_to(exp_local, ROWS)
    groups = seq // ROWS
    move = dff % LANES == 0
    sds = jax.ShapeDtypeStruct
    VM, ANY = pltpu.VMEM, pl.ANY

    ins = dict(
        tokens=tokens,
        state=state,
        gain1=norm_gain[None, :],
        wq=w_query,
        wf=w_forget,
        wi=w_input,
        wo=w_outgate,
        lb=lower_bound[None, :],
        hg=head_gain[None, :],
        wout=w_output,
        gain2=ffn_gain[None, :],
        ids=route_ids.T,
        weights=route_weight.T,
        eg=expert_gate,
        eu=expert_up,
        ed=expert_down,
        sg=shared_gate,
        su=shared_up,
        sd=shared_down,
        mix=dense_mix[None, :],
    )
    if move:
        ins.update(dgate=dense_gate, dup=dense_up, ddown=dense_down)
    else:
        gate_w, up_w = [
            lax.all_to_all(w, "tp", split_axis=1, concat_axis=0, tiled=True)
            for w in (dense_gate, dense_up)
        ]
        down_w = lax.all_to_all(dense_down, "tp", split_axis=0, concat_axis=1, tiled=True)
        ins.update(gatew=gate_w, upw=up_w, downw=down_w)
    outs = dict(out=sds((seq, cols), BF16), new_state=sds(state.shape, F32))
    hops = zs * sides * sides
    scratch = dict(
        tokens_v=VM((seq, width), BF16),
        gain1_v=VM((1, width), F32),
        gain2_v=VM((1, width), F32),
        lb_v=VM((1, mixw), F32),
        hg_v=VM((1, mixw), F32),
        mix_v=VM((1, cols), F32),
        ids_v=VM(route_ids.shape[::-1], jnp.int32),
        weights_v=VM(route_weight.shape[::-1], F32),
        wout_v=VM((mixw, width), BF16),
        st=VM(state.shape, F32),
        nsend=VM((zs * seq, sides * depth), BF16),
        ncol=VM((zs * seq, sides * depth), BF16),
        wbuf=VM((4, sides * depth, mixw), BF16),
        psend=VM((4, zs * seq, mixw), BF16),
        precv=VM((4, zs * seq, mixw), BF16),
        dturn=VM((groups, mixw, ROWS), F32),
        qturn=VM((groups, mixw, ROWS), F32),
        vals=VM((seq, mixw), F32),
        read=VM((seq, mixw), F32),
        rsend=VM((n, rrows, lanes), F32),
        rrecv=VM((n, rrows, lanes), F32),
        mixs=VM((ROWS, cols), F32),
        mixr=VM((tpn, ROWS, cols), F32),
        hsend=VM((tpn, seq, cols), BF16),
        hrecv=VM((tpn, seq, cols), BF16),
        resid=VM((seq, cols), F32),
        rows=VM((CORES, n * seq, half), BF16),
        sqs=VM((ROWS, lanes), F32),
        sqr=VM((tpn, ROWS, lanes), F32),
        scs=VM((ROWS, lanes), F32),
        scr=VM((n, ROWS, lanes), F32),
        egv=VM((CORES, exp_local, half, ff), BF16),
        euv=VM((CORES, exp_local, half, ff), BF16),
        edv=VM((exp_local * ff, width), BF16),
        sgv=VM((CORES, half, sff), BF16),
        suv=VM((CORES, half, sff), BF16),
        sdv=VM((sff, width), BF16),
        dgv=VM((CORES, half, dff), BF16),
        duv=VM((CORES, half, dff), BF16),
        ddv=VM((tpn, dff, cols), BF16),
        acc=VM((2 * exp_local, n * seq, ff), F32),
        dacc=VM((2, n * seq, dff), F32),
        hid=VM((n * seq, exp_local * ff), BF16),
        dhid=VM((n * seq, dff), BF16),
        shared=VM((tpn, seq, cols), F32),
        part=VM((sides, n * seq, cols), BF16),
        crecv=VM((sides, n * seq, cols), BF16),
        both=VM((sides, n * seq, cols), BF16),
        arecv=VM((hops, seq, cols), BF16),
        keep=VM((zs, seq, cols), F32),
        bsend=VM((zs * sides, seq, cols), BF16),
        brecv=VM((zs * sides, seq, cols), BF16),
        zsend=VM((zs, seq, cols), BF16),
        zrecv=VM((zs, seq, cols), BF16),
        local=pltpu.SemaphoreType.DMA((64 + groups + 8 * exp_local * tpn,)),
        stout=pltpu.SemaphoreType.DMA((groups,)),
    )
    counts = {
        WEIGHT: 4 * sides,
        NORMED: zs,
        MOVE: 3 * tpn,
        ROUTE: n,
        MIX: tpn,
        PROJ: 4 * zs,
        HEAD: tpn,
        GATHER_Z: zs,
        GATHER_A: zs * sides,
        GATHER_B: hops,
        GATHER_C: hops,
        SQUARE: tpn,
        SCALE: n,
        SUM_C: sides,
        SUM_A: hops,
        SUM_B: zs * sides,
        SUM_Z: zs,
    }
    names = [*ins, *outs, *scratch]
    sems = [pltpu.SemaphoreType.DMA((counts[k],)) for k in range(len(counts)) for _ in range(2)]
    held = pl.pallas_call(
        functools.partial(layer_kernel, n, tpn, move, names),
        out_shape=tuple(outs.values()),
        in_specs=[pl.BlockSpec(memory_space=ANY) for _ in ins],
        out_specs=(pl.BlockSpec(memory_space=VM), pl.BlockSpec(memory_space=ANY)),
        scratch_shapes=list(scratch.values()) + sems,
        compiler_params=pltpu.CompilerParams(
            collective_id=0, has_side_effects=True, vmem_limit_bytes=VMEM_BYTES
        ),
    )(*ins.values())
    return pl.pallas_call(
        place_kernel,
        out_shape=tuple(outs.values()),
        in_specs=[pl.BlockSpec(memory_space=ANY)] * 2,
        out_specs=(pl.BlockSpec(memory_space=ANY),) * 2,
        scratch_shapes=[
            VM((seq, cols), BF16),
            VM(state.shape, F32),
            pltpu.SemaphoreType.DMA((2, groups + 1)),
        ],
        compiler_params=pltpu.CompilerParams(vmem_limit_bytes=VMEM_BYTES),
    )(*held)


def solution(mesh):
    placed = (
        P("ep", None),
        P("ep", "tp", None, None),
        P(),
        P("ep", "tp"),
        P("ep", "tp"),
        P("ep", "tp"),
        P("ep", "tp"),
        P("tp"),
        P("tp"),
        P("tp", None),
        P(),
        P("ep", None),
        P("ep", None),
        P("ep", None, "tp"),
        P("ep", None, "tp"),
        P("ep", "tp", None),
        P(None, "tp"),
        P(None, "tp"),
        P("tp", None),
        P("tp", "ep"),
        P("tp", "ep"),
        P("ep", "tp"),
        P("tp"),
    )
    return jax.shard_map(
        local,
        mesh=mesh,
        in_specs=placed,
        out_specs=(P("ep", "tp"), P("ep", "tp", None, None)),
        check_vma=False,
    )
```

time: 141 us -> 84.2 us (0.60)
  matrix products: 29.6 us -> 0 us
  other arithmetic: 11.1 us -> 0 us
  Pallas kernels: 93.9 us -> 83.5 us
  local copies, waits for them, and re-layouts: 4.81 us -> 0 us
    dot_general x9 -> x0, matrix products: 29.6 us -> none  [the longest x2 10 us: local(): part = part + jnp.dot(hidden, expert_down[e], preferred_element_type=F32)]
    pallas_call x3 -> x2, Pallas kernels: 93.9 us -> 83.5 us  [the longest x1 77.9 us: local(): pl.pallas_call(functools.partial(layer_kernel, n, tpn, move, names), out_...]
    add x2 -> x0, other arithmetic: 7.14 us -> none  [the longest x1 7.12 us: local(): decay[..., None] * state]
    reduce_sum x2 -> x0, other arithmetic: 1.64 us -> none  [the longest x1 1.51 us: local(): jnp.sum(jnp.where(route_ids[:, :, None] == jnp.arange(slots, dtype=jnp.in...]
    convert_element_type x2 -> x0, other arithmetic: 1.54 us -> none  [the longest x1 0.91 us: local(): projected.astype(F32)]
    split x2 -> x0, local copies, waits for them, and re-layouts: 1.48 us -> none  [local(): jnp.split(projected.astype(F32), 4, axis=1)]
    unnamed x13 -> x0, local copies, waits for them, and re-layouts: 1.46 us -> none
where the time goes in v1:
time: 84.2 us; the launch traced here: 84.1 us
  Pallas kernels  83.5 us (99%)
    pallas_call x1, Pallas kernels, local(): pl.pallas_call(functools.partial(layer_kernel, n, tpn, move, names), out_...  77.9 us
    pallas_call x1, Pallas kernels, local(): pl.pallas_call(place_kernel, out_shape=tuple(outs.values()), in_specs=[pl...  5.52 us

profile of v1, /device:TPU:0, one launch (start us, length us, event | category | flops | bytes accessed | tf_op | source)
XLA Modules:
  0.0 84.1 jit_solution(10079552753915666437)
XLA Ops:
  0.6 77.9 %shard_map.230 = (bf16[48,512]{1,0:T(8,128)(2,1)}, f32[48,2,128,128]{3,2,1,0:T(8,128)}) custom-call(bf16[48,2048]{1,0:T(8,128)(2,1)} %refs_0_.1, f32[48,2,128,128]{3,2,1,0:T(8,128)} %refs_1_.1, f32[1,2048]{1,0:T(1,128)} %bitcast.7, bf16[256,256]{1,0:T(8,128)(2,1)} %refs_3_.1, bf16[256,256]{1,0:T(8,128)(2,1)} %refs_4_.1, bf16[256,256]{1,0:T(8,128)(2,1)} %refs_5_.1, ...), custom_call_target="tpu_custom_call" | custom-call | tf_op jit(solution)/shard_map/pallas_call | solution.py:751
  78.6 5.5 %shard_map.231 = (bf16[48,512]{1,0:T(8,128)(2,1)}, f32[48,2,128,128]{3,2,1,0:T(8,128)}) custom-call(bf16[48,512]{1,0:T(8,128)(2,1)} %get-tuple-element.4.held, f32[48,2,128,128]{3,2,1,0:T(8,128)} %get-tuple-element.5.held_state), custom_call_target="tpu_custom_call" | custom-call | tf_op jit(solution)/shard_map/pallas_call | solution.py:761

commit v2 on v1

v2 whole, which is shorter than its diff:
```python
import functools
import types

import jax
import jax.numpy as jnp
from jax import lax
from jax.experimental import pallas as pl
from jax.experimental.pallas import tpu as pltpu
from jax.sharding import PartitionSpec as P

EPS = 1e-06
LANES = 128
CORES = 2
ROWS = 8
F32 = jnp.float32
BF16 = jnp.bfloat16
PIECES = 4
AHEAD = (13, 2)
PLACE_BYTES = 1024 * 1024
VMEM_BYTES = 52 * 1024 * 1024
(
    WEIGHT,
    NORMED,
    MOVE,
    ROUTE,
    HIDDEN_Y,
    HIDDEN_C,
    PROJ,
    HEAD,
    GATHER_Z,
    GATHER_A,
    GATHER_B,
    GATHER_C,
    SQUARE,
    SCALE,
    SUM_C,
    SUM_Y,
    SUM_X,
    SUM_Z,
) = range(18)


def span(index, size):
    if isinstance(index, int):
        return pl.ds(index * size, size)
    return pl.ds(pl.multiple_of(index * size, size), size)


def ceil_to(value, step):
    return -(-value // step) * step


def silu(v):
    return v * jax.nn.sigmoid(v)


def schedule(zs):
    Z, FIRST, SECOND, HALF, DENSE, EXPERT, DOWN, TWIN, HIDDEN, SUMS_Y, SUMS_X, SCALES, STATE = range(13)
    cost = (0.05, 0.05, 0.08, 0.5, 0.4, 0.6, 0.4, 0.53, 0.05, 0.37, 0.05, 0.1, 2.6)
    relays = (Z, FIRST, SECOND, SCALES, HIDDEN)
    after = {(STATE, 0): [], (SCALES, 0): [(None, 2.8)]}
    for k in range(zs):
        after[Z, k] = [(None, 2.8 + 1.6 * k if k else 0.0)]
        after[FIRST, k] = [((Z, k), 2.5)]
        after[SECOND, k] = [((FIRST, k), 2.5)]
        after[HALF, k] = [((SECOND, k), 0.0)]
        after[DENSE, k] = [((SECOND, k), 1.4), ((HALF, k), 0.0), ((SCALES, 0), 2.5)]
        after[EXPERT, k] = [((DENSE, k), 0.0)]
        after[DOWN, k] = [((EXPERT, k), 0.0)]
        after[TWIN, k] = [((DOWN, k), 1.4)]
        after[HIDDEN, k] = [((DENSE, k), 2.6)]
        after[SUMS_Y, k] = [((TWIN, k), 3.7), ((HIDDEN, k), 1.3)]
        after[SUMS_X, k] = [((SUMS_Y, k), 2.7)]
    done, now, order = {(Z, 0): 0.0, None: 0.0}, 0.0, []
    del after[Z, 0]
    while after:
        ready = {
            step: max([done[need] + wait for need, wait in needs] or [0.0])
            for step, needs in after.items()
            if all(need in done for need, _ in needs)
        }
        now = max(now, min(ready.values()))
        step = min(
            (step for step, at in ready.items() if at <= now),
            key=lambda step: (step[0] not in relays, step[0] == STATE, -step[0], step[1]),
        )
        now += cost[step[0]] + (0.8 if step == (DOWN, 0) else 0.0)
        done[step] = now
        order.append(step)
        del after[step]
    return order


def layer_kernel(n, tpn, move, names, *refs):
    sems = refs[len(names) :]
    r = types.SimpleNamespace(**dict(zip(names, refs)))
    me, tp = lax.axis_index("ep"), lax.axis_index("tp")
    sides = tpn // CORES
    xs = sides
    zs = n // xs
    z, x = lax.div(me, xs), lax.rem(me, xs)
    y, c = lax.div(tp, CORES), lax.rem(tp, CORES)
    twin_core = CORES - 1 - c
    seq, width = r.tokens.shape
    cols = width // tpn
    depth, mixw = r.wq.shape
    exp_local, _, ff = r.eg.shape
    sff = r.sg.shape[1]
    dff = r.dgv.shape[2]
    heads, hd = r.state.shape[1:3]
    wrap = xs * depth
    lanes = r.sqs.shape[1]
    half = sides * cols

    def pick(first, second):
        return first * (1 - c) + second * c

    def device(zz, xx, yy, cc):
        return {"ep": zz * xs + xx, "tp": yy * CORES + cc}

    waiting = []

    def send(src, dst, kind, slot, peer, landing=None):
        copy = pltpu.make_async_remote_copy(
            src_ref=src,
            dst_ref=dst,
            send_sem=sems[2 * kind].at[slot],
            recv_sem=sems[2 * kind + 1].at[slot if landing is None else landing],
            device_id=peer,
            device_id_type=pl.DeviceIdType.MESH,
        )
        copy.start()
        waiting.append(copy)
        return copy

    def landed(kind, slot, ref):
        pltpu.make_async_remote_copy(
            src_ref=ref,
            dst_ref=ref,
            send_sem=sems[2 * kind].at[slot],
            recv_sem=sems[2 * kind + 1].at[slot],
            device_id=device(z, x, y, twin_core),
            device_id_type=pl.DeviceIdType.MESH,
        ).wait_recv()

    high = lax.div(2 * z, zs)
    near = z * (1 - high) + (zs - 1 - z) * high

    def zat(k):
        if k == 0:
            return z
        place = k - 1 + lax.div(zs + k - 1 - near, zs)
        return place * (1 - high) + (zs - 1 - place) * high

    far_first = range(zs - 1, 0, -1)
    used = [0]

    def fetch(src, dst):
        copy = pltpu.make_async_copy(src, dst, r.local.at[used[0]])
        used[0] += 1
        copy.start()
        return copy

    got = types.SimpleNamespace()
    got.tokens = fetch(r.tokens, r.tokens_v)
    got.gain1 = fetch(r.gain1, r.gain1_v)
    order = (r.wf, r.wq, r.wi, r.wo)
    got.w = [fetch(w, r.wbuf.at[i, span(x, depth), :]) for i, w in enumerate(order)]
    got.lb = fetch(r.lb, r.lb_v)
    got.hg = fetch(r.hg, r.hg_v)
    got.mix = fetch(r.mix, r.mix_v)
    got.ids = fetch(r.ids, r.ids_v)
    got.weights = fetch(r.weights, r.weights_v)
    groups = seq // ROWS
    states = [
        fetch(r.state.at[pl.ds(g * ROWS, ROWS)], r.new_state.at[pl.ds(g * ROWS, ROWS)])
        for g in range(groups)
    ]
    got.wout = fetch(r.wout, r.wout_v)
    got.gain2 = fetch(r.gain2, r.gain2_v)

    barrier = pltpu.get_barrier_semaphore()
    for s in range(1, tpn):
        pl.semaphore_signal(
            barrier,
            inc=1,
            device_id={"tp": lax.rem(tp + s, tpn)},
            device_id_type=pl.DeviceIdType.MESH,
        )
    for s in range(1, n):
        pl.semaphore_signal(
            barrier,
            inc=1,
            device_id={"ep": lax.rem(me + s, n)},
            device_id_type=pl.DeviceIdType.MESH,
        )
    got.tokens.wait()
    got.gain1.wait()
    t32 = r.tokens_v[...].astype(F32)
    normed = (
        t32 * lax.rsqrt(jnp.mean(t32 * t32, axis=-1, keepdims=True) + EPS) * r.gain1_v[...]
    ).astype(BF16)
    for d in range(zs):
        r.nsend[d * seq : (d + 1) * seq, :] = normed[:, d * wrap : (d + 1) * wrap]
    r.ncol[span(z, seq), :] = r.nsend[span(z, seq), :]
    pl.semaphore_wait(barrier, n - 1 + tpn - 1)

    arrived = {}
    for i, w in enumerate(order):
        for s in range(1, xs):
            arrived[WEIGHT, i, s] = send(
                w,
                r.wbuf.at[i, span(x, depth), :],
                WEIGHT,
                i * xs + s,
                device(z, lax.rem(x + s, xs), y, c),
            )
    for k in far_first:
        zz = zat(k)
        send(
            r.nsend.at[span(zz, seq)],
            r.ncol.at[span(z, seq)],
            NORMED,
            k,
            device(zz, x, y, c),
            z,
        )
    pieces = []
    if move:
        rows = r.dgate.shape[0]
        got.dgv = []
        for i, (src, dst) in enumerate(((r.dgate, r.dgv), (r.dup, r.duv))):
            for q in range(sides):
                for k in range(CORES):
                    core = twin_core if k else c
                    peer = lax.rem(y + q, sides) * CORES + core
                    count = PIECES if q else 1
                    size = rows // count
                    for j in range(count):
                        part = pl.ds(j * size, size)
                        a = src.at[part, span(peer, dff)]
                        b = dst.at[c, pl.ds(pl.multiple_of(y * rows + j * size, ROWS), size), :]
                        slot = ((i * sides + q) * CORES + k) * PIECES + j
                        if q:
                            pieces.append((a, b, slot, peer, i))
                        elif k:
                            arrived[MOVE, i, slot] = send(a, b, MOVE, slot, {"tp": peer})
                        else:
                            got.dgv.append(fetch(a, b))

    def move_pieces(count):
        for a, b, slot, peer, i in pieces[:count]:
            arrived[MOVE, i, slot] = send(a, b, MOVE, slot, {"tp": peer})
        del pieces[:count]

    def moved():
        for key, copy in arrived.items():
            if key[0] == MOVE:
                copy.wait_recv()

    move_pieces(AHEAD[0])

    got.ids.wait()
    got.weights.wait()
    got.mix.wait()
    eye = lax.broadcasted_iota(jnp.int32, (seq, lanes), 0) == lax.broadcasted_iota(
        jnp.int32, (seq, lanes), 1
    )
    ids, weights = r.ids_v[...], r.weights_v[...]
    rrows = r.rsend.shape[1]

    def to_row(col):
        return jnp.sum(jnp.where(eye, col, 0.0), axis=0, keepdims=True)

    def to_col(row):
        return jnp.sum(jnp.where(eye, row, 0.0), axis=1, keepdims=True)

    for d in range(n):
        r.rsend[d] = jnp.zeros((rrows, lanes), F32)
        for i in range(exp_local):
            r.rsend[d, i : i + 1, :seq] = jnp.sum(
                jnp.where(ids == d * exp_local + i, weights, 0.0), axis=0, keepdims=True
            )
    r.rrecv[me] = r.rsend[me]
    for s in range(1, n):
        peer = lax.rem(me + s, n)
        arrived[ROUTE, s] = send(
            r.rsend.at[peer], r.rrecv.at[me], ROUTE, s, {"ep": peer}
        )
    def fetch_rows(src, dst):
        return [
            fetch(src.at[span(t, cols), :], dst(t % CORES).at[span(t // CORES, cols), :])
            for t in range(tpn)
        ]

    got.sgv = fetch_rows(r.sg, lambda k: r.sgv.at[k]) + fetch_rows(r.su, lambda k: r.suv.at[k])
    got.sdv = [fetch(r.sd, r.sdv)]
    got.egv = []
    for e in range(exp_local):
        got.egv += fetch_rows(r.eg.at[e], lambda k: r.egv.at[k, e])
        got.egv += fetch_rows(r.eu.at[e], lambda k: r.euv.at[k, e])
    got.edv = [fetch(r.ed.at[e], r.edv.at[span(e, ff), :]) for e in range(exp_local)]
    got.ddv = fetch(r.ddown, r.ddv)
    if not move:
        got.dgv = fetch_rows(r.gatew, lambda k: r.dgv.at[k])
        got.dgv += fetch_rows(r.upw, lambda k: r.duv.at[k])

    for k in range(1, zs):
        landed(NORMED, zat(k), r.ncol.at[span(zat(k), seq)])
    for i in range(len(order)):
        got.w[i].wait()
        for s in range(1, xs):
            arrived[WEIGHT, i, s].wait_recv()
        r.psend[i] = jnp.dot(
            r.ncol[...], r.wbuf[i], preferred_element_type=F32
        ).astype(BF16)
        for k in far_first:
            zz = zat(k)
            send(
                r.psend.at[i, span(zz, seq)],
                r.precv.at[i, span(z, seq)],
                PROJ,
                i * zs + k,
                device(zz, x, y, c),
                i * zs + z,
            )

    def projected(i):
        total = r.psend[i, span(z, seq), :].astype(F32)
        for k in range(1, zs):
            zz = zat(k)
            landed(PROJ, i * zs + zz, r.precv.at[i, span(zz, seq)])
            total = total + r.precv[i, span(zz, seq), :].astype(F32)
        return total.astype(BF16).astype(F32)

    padded = ceil_to(seq, LANES)

    def turn(value, dst):
        if padded > seq:
            value = jnp.concatenate([value, jnp.zeros((padded - seq, mixw), F32)], axis=0)
        value = value.T
        for g in range(groups):
            dst[g] = value[:, g * ROWS : (g + 1) * ROWS]

    got.lb.wait()
    got.hg.wait()
    lb = r.lb_v[...]
    decay = lb + (1.0 - lb) * jax.nn.sigmoid(projected(0))
    query = projected(1)
    turn(decay, r.dturn)
    turn(query * decay, r.qturn)
    keyed = query * (1.0 - decay)
    for copy in states:
        copy.wait()

    def read_group(g, carry):
        qg = r.qturn[g]
        rows = []
        for b in range(ROWS):
            parts = [
                jnp.sum(
                    qg[h * hd : (h + 1) * hd, b : b + 1] * r.new_state[g * ROWS + b, h],
                    axis=0,
                    keepdims=True,
                )
                for h in range(heads)
            ]
            rows.append(jnp.concatenate(parts, axis=1))
        r.read[span(g, ROWS), :] = jnp.concatenate(rows, axis=0)
        return carry

    lax.fori_loop(0, groups, read_group, 0)

    def write_group(g, carry):
        dg = r.dturn[g]
        vg = r.vals[span(g, ROWS), :]
        for b in range(ROWS):
            for h in range(heads):
                at = slice(h * hd, (h + 1) * hd)
                vrow = vg[b : b + 1, at]
                old = r.new_state[g * ROWS + b, h]
                r.new_state[g * ROWS + b, h] = vrow + dg[at, b : b + 1] * (old - vrow)
        return carry

    values = projected(2)
    r.vals[...] = values
    read = r.read[...]
    parts = []
    for h in range(heads):
        at = slice(h * hd, (h + 1) * hd)
        part = read[:, at] + jnp.sum(keyed[:, at], axis=-1, keepdims=True) * values[:, at]
        parts.append(part * lax.rsqrt(jnp.mean(part * part, axis=-1, keepdims=True) + EPS))
    read = jnp.concatenate(parts, axis=1)
    head = (read * r.hg_v[...] * silu(projected(3))).astype(BF16)

    got.wout.wait()
    got.gain2.wait()
    for t in range(tpn):
        r.hsend[t] = jnp.dot(
            head, r.wout_v[:, t * cols : (t + 1) * cols], preferred_element_type=F32
        ).astype(BF16)
    for s in range(1, tpn):
        peer = lax.rem(tp + s, tpn)
        arrived[HEAD, s] = send(r.hsend.at[peer], r.hrecv.at[tp], HEAD, s, {"tp": peer})
    move_pieces(AHEAD[1])
    mine = span(tp, cols)
    total = r.tokens_v[:, mine].astype(F32) + r.hsend[tp].astype(F32)
    for s in range(1, tpn):
        arrived[HEAD, s].wait_recv()
        total = total + r.hrecv[lax.rem(tp + tpn - s, tpn)].astype(F32)
    r.resid[...] = total

    def block(zz, xx, yy, cc):
        return r.rows.at[cc, span(zz * xs + xx, seq), span(yy, cols)]

    r.rows[c, span(me, seq), span(y, cols)] = (total * r.gain2_v[:, mine]).astype(BF16)
    own = block(z, x, y, c)
    for k in far_first:
        send(own, own, GATHER_Z, k, device(zat(k), x, y, c), z)

    def plane(k, a, b):
        xx = lax.rem(x + xs - pick(a, b), xs)
        yy = lax.rem(y + sides - pick(b, a), sides)
        return block(zat(k), xx, yy, c)

    def forward_first(k):
        ref = plane(k, 0, 0)
        for q in range(1, sides):
            peer = device(z, lax.rem(x + pick(q, 0), xs), lax.rem(y + pick(0, q), sides), c)
            arrived[GATHER_A, k, q] = send(ref, ref, GATHER_A, k * sides + q, peer)

    def forward_second(k, a):
        ref = plane(k, a, 0)
        for q in range(1, sides):
            peer = device(z, lax.rem(x + pick(0, q), xs), lax.rem(y + pick(q, 0), sides), c)
            arrived[GATHER_B, k, a, q] = send(
                ref, ref, GATHER_B, (k * sides + a) * sides + q, peer
            )

    def forward_twin(k, a, b):
        ref = plane(k, a, b)
        arrived[GATHER_C, k, a, b] = send(
            ref, ref, GATHER_C, (k * sides + a) * sides + b, device(z, x, y, twin_core)
        )

    forward_first(0)
    forward_second(0, 0)
    forward_twin(0, 0, 0)
    move_pieces(len(pieces))

    square = to_row(jnp.sum(total * total, axis=-1, keepdims=True))
    r.sqs[...] = jnp.broadcast_to(square, (ROWS, lanes))
    for s in range(1, tpn):
        arrived[SQUARE, s] = send(
            r.sqs, r.sqr.at[tp], SQUARE, s, {"tp": lax.rem(tp + s, tpn)}
        )
    size = xs * seq
    pairs = [(r.egv, r.euv, e) for e in range(exp_local)] + [(r.dgv, r.duv, None)]

    def weight(ref, lead, core):
        return ref[core] if lead is None else ref[core, lead]

    def scale_out(k):
        square = r.sqs[:1]
        for s in range(1, tpn):
            arrived[SQUARE, s].wait_recv()
            square = square + r.sqr[lax.rem(tp + tpn - s, tpn)][:1]
        r.scr[me] = jnp.broadcast_to(lax.rsqrt(square / width + EPS), (ROWS, lanes))
        for s in range(1, n):
            send(r.scr.at[me], r.scr.at[me], SCALE, s, {"ep": lax.rem(me + s, n)}, me)

    def from_z(k):
        landed(GATHER_Z, zat(k), plane(k, 0, 0))
        forward_first(k)
        forward_second(k, 0)
        forward_twin(k, 0, 0)

    def from_first(k):
        for a in range(1, sides):
            arrived[GATHER_A, k, a].wait_recv()
            forward_second(k, a)
            forward_twin(k, a, 0)

    def from_second(k):
        for a in range(sides):
            for b in range(1, sides):
                arrived[GATHER_B, k, a, b].wait_recv()
                forward_twin(k, a, b)

    def first_half(k):
        if k == 0:
            for copy in got.egv + got.dgv:
                copy.wait()
            moved()
        lhs = r.rows[c, span(zat(k), size), :]
        for i, (gate, up, lead) in enumerate(pairs):
            for j, ref in enumerate((gate, up)):
                product = jnp.dot(lhs, weight(ref, lead, c), preferred_element_type=F32)
                if lead is None:
                    r.dacc[j, k] = product
                else:
                    r.acc[2 * i + j, k] = product

    def column(ref, k, row):
        return jnp.concatenate(
            [to_col(ref[zat(k) * xs + i][row : row + 1]) for i in range(xs)], axis=0
        )

    def shared_expert():
        for copy in got.sgv + got.sdv:
            copy.wait()
        pre = [
            sum(
                jnp.dot(r.rows[k, span(me, seq), :], ref[k], preferred_element_type=F32)
                for k in range(CORES)
            )
            for ref in (r.sgv, r.suv)
        ]
        own_scale = to_col(r.scr[me][:1])
        hidden = (silu(own_scale * pre[0]) * (own_scale * pre[1])).astype(BF16)
        for t in range(tpn):
            r.shared[t] = jnp.dot(
                hidden, r.sdv[:, t * cols : (t + 1) * cols], preferred_element_type=F32
            )

    def partial(k, yy, cc):
        t = yy * CORES + cc
        value = jnp.dot(r.hid[k], r.edv[:, span(t, cols)], preferred_element_type=F32)
        if k == 0:
            r.wide[...] = value
            r.wide[span(x, seq), :] = r.wide[span(x, seq), :] + r.shared[t]
            value = r.wide[...]
        return value

    def dense_half(k):
        for a in range(sides):
            for b in range(sides):
                arrived[GATHER_C, k, a, b].wait_recv()
        if k == 0:
            for s in range(1, n):
                arrived[ROUTE, s].wait_recv()
        for i in range(xs):
            if k or i:
                e = zat(k) * xs + lax.rem(x + i, xs)
                landed(SCALE, e, r.scr.at[e])
        hidden_of(k, len(pairs) - 1)

    def expert_half(k):
        for i in range(exp_local):
            hidden_of(k, i)

    def hidden_of(k, i):
        scale = column(r.scr, k, 0)
        lhs = r.rows[twin_core, span(zat(k), size), :]
        gate, up, lead = pairs[i]
        both = []
        for j, ref in enumerate((gate, up)):
            before = r.dacc[j, k] if lead is None else r.acc[2 * i + j, k]
            product = jnp.dot(lhs, weight(ref, lead, twin_core), preferred_element_type=F32)
            both.append(scale * (before + product))
        hidden = silu(both[0]) * both[1]
        if lead is None:
            r.dhid[k, tp] = hidden.astype(BF16)
            ref = r.dhid.at[k, tp]
            for q in range(1, sides):
                peer = device(z, x, lax.rem(y + q, sides), c)
                arrived[HIDDEN_Y, k, q] = send(ref, ref, HIDDEN_Y, k * sides + q, peer)
            arrived[HIDDEN_C, k, 0] = send(
                ref, ref, HIDDEN_C, k * sides, device(z, x, y, twin_core)
            )
        else:
            share = column(r.rrecv, k, lead)
            r.hid[k, :, i * ff : (i + 1) * ff] = (hidden * share).astype(BF16)

    def down(k):
        if k == 0:
            for copy in got.edv:
                copy.wait()
            shared_expert()
        for q in [*range(1, sides), 0]:
            slot = k * sides + q
            r.part[slot] = partial(k, lax.rem(y + q, sides), twin_core).astype(BF16)
            arrived[SUM_C, k, q] = send(
                r.part.at[slot], r.crecv.at[slot], SUM_C, slot, device(z, x, y, twin_core)
            )

    def hidden_on(k):
        for q in range(1, sides):
            arrived[HIDDEN_Y, k, q].wait_recv()
            ref = r.dhid.at[k, lax.rem(y + sides - q, sides) * CORES + c]
            arrived[HIDDEN_C, k, q] = send(
                ref, ref, HIDDEN_C, k * sides + q, device(z, x, y, twin_core)
            )

    def from_twin(k):
        for q in [*range(1, sides), 0]:
            slot = k * sides + q
            yy = lax.rem(y + q, sides)
            value = partial(k, yy, c)
            arrived[SUM_C, k, q].wait_recv()
            value = value + r.crecv[slot].astype(F32)
            if q == 0:
                r.keep[k] = value
                continue
            r.ysend[slot] = value.astype(BF16)
            arrived[SUM_Y, k, q] = send(
                r.ysend.at[slot], r.yrecv.at[slot], SUM_Y, slot, device(z, x, yy, c)
            )

    def from_y(k):
        for q in range(sides):
            arrived[HIDDEN_C, k, q].wait_recv()
        if k == 0:
            got.ddv.wait()
        dense = sum(
            jnp.dot(
                r.dhid[k, t], r.ddv[t * dff : (t + 1) * dff, :], preferred_element_type=F32
            )
            for t in range(tpn)
        )
        value = r.keep[k] + jax.nn.sigmoid(r.mix_v[...]) * dense
        for q in range(1, sides):
            arrived[SUM_Y, k, q].wait_recv()
            value = value + r.yrecv[k * sides + q].astype(F32)
        r.keep[k] = value
        for q in range(1, xs):
            slot = k * sides + q
            xx = lax.rem(x + q, xs)
            r.xsend[slot] = r.keep[k, span(xx, seq), :].astype(BF16)
            arrived[SUM_X, k, q] = send(
                r.xsend.at[slot], r.xrecv.at[slot], SUM_X, slot, device(z, xx, y, c)
            )

    def from_x(k):
        value = r.keep[k, span(x, seq), :]
        for q in range(1, xs):
            arrived[SUM_X, k, q].wait_recv()
            value = value + r.xrecv[k * sides + q].astype(F32)
        if k == 0:
            r.resid[...] = r.resid[...] + value
        else:
            r.zsend[k] = value.astype(BF16)
            send(r.zsend.at[k], r.zrecv.at[z], SUM_Z, k, device(zat(k), x, y, c), z)

    def write_state(k):
        lax.fori_loop(0, groups, write_group, 0)

    kinds = (
        from_z, from_first, from_second, first_half, dense_half, expert_half, down,
        from_twin, hidden_on, from_y, from_x, scale_out, write_state,
    )
    for kind, k in schedule(zs):
        step = kinds[kind]
        step(k)

    final = r.resid[...]
    for k in range(1, zs):
        landed(SUM_Z, zat(k), r.zrecv.at[zat(k)])
        final = final + r.zrecv[zat(k)].astype(F32)
    r.out[...] = final.astype(BF16)

    for copy in waiting:
        copy.wait_send()


def place_kernel(held, held_state, out, new_state, sems):
    parts = [pl.ds(g * ROWS, ROWS) for g in range(held_state.shape[0] // ROWS)]
    moves = [(held_state.at[p], new_state.at[p]) for p in parts] + [(held, out)]
    copies = [pltpu.make_async_copy(*move, sems.at[k]) for k, move in enumerate(moves)]
    for copy in copies:
        copy.start()
    for copy in copies:
        copy.wait()


def local(
    tokens,
    state,
    norm_gain,
    w_query,
    w_forget,
    w_input,
    w_outgate,
    lower_bound,
    head_gain,
    w_output,
    ffn_gain,
    route_ids,
    route_weight,
    expert_gate,
    expert_up,
    expert_down,
    shared_gate,
    shared_up,
    shared_down,
    dense_gate,
    dense_up,
    dense_down,
    dense_mix,
):
    n = lax.axis_size("ep")
    tpn = lax.axis_size("tp")
    sides = tpn // CORES
    zs = n // sides
    seq, width = tokens.shape
    depth, mixw = w_query.shape
    heads, hd = state.shape[1:3]
    cols = width // tpn
    half = sides * cols
    exp_local, _, ff = expert_gate.shape
    sff = shared_gate.shape[1]
    dff = dense_gate.shape[1] // tpn
    lanes = ceil_to(seq, LANES)
    rrows = ceil_to(exp_local, ROWS)
    groups = seq // ROWS
    move = dff % LANES == 0
    sds = jax.ShapeDtypeStruct
    VM, ANY = pltpu.VMEM, pl.ANY

    ins = dict(
        tokens=tokens,
        state=state,
        gain1=norm_gain[None, :],
        wq=w_query,
        wf=w_forget,
        wi=w_input,
        wo=w_outgate,
        lb=lower_bound[None, :],
        hg=head_gain[None, :],
        wout=w_output,
        gain2=ffn_gain[None, :],
        ids=route_ids.T,
        weights=route_weight.T,
        eg=expert_gate,
        eu=expert_up,
        ed=expert_down,
        sg=shared_gate,
        su=shared_up,
        sd=shared_down,
        mix=dense_mix[None, :],
        ddown=dense_down,
    )
    if move:
        ins.update(dgate=dense_gate, dup=dense_up)
    else:
        gate_w, up_w = [
            lax.all_to_all(w, "tp", split_axis=1, concat_axis=0, tiled=True)
            for w in (dense_gate, dense_up)
        ]
        ins.update(gatew=gate_w, upw=up_w)
    outs = dict(out=sds((seq, cols), BF16), new_state=sds(state.shape, F32))
    hops = zs * sides * sides
    size = sides * seq
    scratch = dict(
        tokens_v=VM((seq, width), BF16),
        gain1_v=VM((1, width), F32),
        gain2_v=VM((1, width), F32),
        lb_v=VM((1, mixw), F32),
        hg_v=VM((1, mixw), F32),
        mix_v=VM((1, cols), F32),
        ids_v=VM(route_ids.shape[::-1], jnp.int32),
        weights_v=VM(route_weight.shape[::-1], F32),
        wout_v=VM((mixw, width), BF16),
        nsend=VM((zs * seq, sides * depth), BF16),
        ncol=VM((zs * seq, sides * depth), BF16),
        wbuf=VM((4, sides * depth, mixw), BF16),
        psend=VM((4, zs * seq, mixw), BF16),
        precv=VM((4, zs * seq, mixw), BF16),
        dturn=VM((groups, mixw, ROWS), F32),
        qturn=VM((groups, mixw, ROWS), F32),
        vals=VM((seq, mixw), F32),
        read=VM((seq, mixw), F32),
        rsend=VM((n, rrows, lanes), F32),
        rrecv=VM((n, rrows, lanes), F32),
        hsend=VM((tpn, seq, cols), BF16),
        hrecv=VM((tpn, seq, cols), BF16),
        resid=VM((seq, cols), F32),
        rows=VM((CORES, n * seq, half), BF16),
        sqs=VM((ROWS, lanes), F32),
        sqr=VM((tpn, ROWS, lanes), F32),
        scr=VM((n, ROWS, lanes), F32),
        egv=VM((CORES, exp_local, half, ff), BF16),
        euv=VM((CORES, exp_local, half, ff), BF16),
        edv=VM((exp_local * ff, width), BF16),
        sgv=VM((CORES, half, sff), BF16),
        suv=VM((CORES, half, sff), BF16),
        sdv=VM((sff, width), BF16),
        dgv=VM((CORES, half, dff), BF16),
        duv=VM((CORES, half, dff), BF16),
        ddv=VM(dense_down.shape, BF16),
        acc=VM((2 * exp_local, zs, size, ff), F32),
        dacc=VM((2, zs, size, dff), F32),
        hid=VM((zs, size, exp_local * ff), BF16),
        dhid=VM((zs, tpn, size, dff), BF16),
        wide=VM((size, cols), F32),
        part=VM((zs * sides, size, cols), BF16),
        crecv=VM((zs * sides, size, cols), BF16),
        ysend=VM((zs * sides, size, cols), BF16),
        yrecv=VM((zs * sides, size, cols), BF16),
        keep=VM((zs, size, cols), F32),
        xsend=VM((zs * sides, seq, cols), BF16),
        xrecv=VM((zs * sides, seq, cols), BF16),
        zsend=VM((zs, seq, cols), BF16),
        zrecv=VM((zs, seq, cols), BF16),
        shared=VM((tpn, seq, cols), F32),
        local=pltpu.SemaphoreType.DMA((64 + groups + 8 * exp_local * tpn,)),
    )
    counts = {
        WEIGHT: 4 * sides,
        NORMED: zs,
        MOVE: 2 * tpn * PIECES,
        ROUTE: n,
        HIDDEN_Y: zs * sides,
        HIDDEN_C: zs * sides,
        PROJ: 4 * zs,
        HEAD: tpn,
        GATHER_Z: zs,
        GATHER_A: zs * sides,
        GATHER_B: hops,
        GATHER_C: hops,
        SQUARE: tpn,
        SCALE: n,
        SUM_C: zs * sides,
        SUM_Y: zs * sides,
        SUM_X: zs * sides,
        SUM_Z: zs,
    }
    names = [*ins, *outs, *scratch]
    sems = [pltpu.SemaphoreType.DMA((counts[k],)) for k in range(len(counts)) for _ in range(2)]
    held = pl.pallas_call(
        functools.partial(layer_kernel, n, tpn, move, names),
        out_shape=tuple(VM(out.shape, out.dtype) for out in outs.values()),
        in_specs=[pl.BlockSpec(memory_space=ANY) for _ in ins],
        out_specs=(pl.BlockSpec(memory_space=VM),) * 2,
        scratch_shapes=list(scratch.values()) + sems,
        compiler_params=pltpu.CompilerParams(
            collective_id=0, has_side_effects=True, vmem_limit_bytes=VMEM_BYTES
        ),
    )(*ins.values())
    return pl.pallas_call(
        place_kernel,
        out_shape=tuple(outs.values()),
        in_specs=[pl.BlockSpec(memory_space=VM)] * 2,
        out_specs=(pl.BlockSpec(memory_space=ANY),) * 2,
        scratch_shapes=[pltpu.SemaphoreType.DMA((groups + 1,))],
        compiler_params=pltpu.CompilerParams(vmem_limit_bytes=PLACE_BYTES),
    )(*[pltpu.with_memory_space_constraint(a, VM) for a in held])


def solution(mesh):
    placed = (
        P("ep", None),
        P("ep", "tp", None, None),
        P(),
        P("ep", "tp"),
        P("ep", "tp"),
        P("ep", "tp"),
        P("ep", "tp"),
        P("tp"),
        P("tp"),
        P("tp", None),
        P(),
        P("ep", None),
        P("ep", None),
        P("ep", None, "tp"),
        P("ep", None, "tp"),
        P("ep", "tp", None),
        P(None, "tp"),
        P(None, "tp"),
        P("tp", None),
        P("tp", "ep"),
        P("tp", "ep"),
        P("ep", "tp"),
        P("tp"),
    )
    return jax.shard_map(
        local,
        mesh=mesh,
        in_specs=placed,
        out_specs=(P("ep", "tp"), P("ep", "tp", None, None)),
        check_vma=False,
    )
```

time: 84.2 us -> 70.3 us (0.83)
  Pallas kernels: 83.5 us -> 69.5 us
    pallas_call x1, Pallas kernels: 77.9 us -> 66.7 us  [local(): pl.pallas_call(functools.partial(layer_kernel, n, tpn, move, names), out_...]
    pallas_call x1, Pallas kernels: 5.52 us -> 2.73 us  [local(): pl.pallas_call(place_kernel, out_shape=tuple(outs.values()), in_specs=[pl...]
where the time goes in v2:
time: 70.3 us; the launch traced here: 70.1 us
  Pallas kernels  69.5 us (99%)
    pallas_call x1, Pallas kernels, local(): pl.pallas_call(functools.partial(layer_kernel, n, tpn, move, names), out_...  66.7 us
    pallas_call x1, Pallas kernels, local(): pl.pallas_call(place_kernel, out_shape=tuple(outs.values()), in_specs=[pl...  2.73 us

profile of v2, /device:TPU:0, one launch (start us, length us, event | category | flops | bytes accessed | tf_op | source)
XLA Modules:
  0.0 70.1 jit_solution(3185434942565338088)
XLA Ops:
  0.6 66.7 %shard_map.230 = (bf16[48,512]{1,0:T(8,128)(2,1)S(1)}, f32[48,2,128,128]{3,2,1,0:T(8,128)S(1)}) custom-call(bf16[48,2048]{1,0:T(8,128)(2,1)} %refs_0_.1, f32[48,2,128,128]{3,2,1,0:T(8,128)} %refs_1_.1, f32[1,2048]{1,0:T(1,128)} %bitcast.7, bf16[256,256]{1,0:T(8,128)(2,1)} %refs_3_.1, bf16[256,256]{1,0:T(8,128)(2,1)} %refs_4_.1, bf16[256,256]{1,0:T(8,128)(2,1)} %refs_5_.1, ...), custom_call_target="tpu_custom_call" | custom-call | tf_op jit(solution)/shard_map/pallas_call | solution.py:830
  67.4 2.7 %shard_map.231 = (bf16[48,512]{1,0:T(8,128)(2,1)}, f32[48,2,128,128]{3,2,1,0:T(8,128)}) custom-call(bf16[48,512]{1,0:T(8,128)(2,1)S(1)} %get-tuple-element.4.held, f32[48,2,128,128]{3,2,1,0:T(8,128)S(1)} %get-tuple-element.5.held_state), custom_call_target="tpu_custom_call" | custom-call | tf_op jit(solution)/shard_map/pallas_call | solution.py:840

commit v3 on v2

--- a/solution.py
+++ b/solution.py
@@ -15,7 +15,8 @@
 F32 = jnp.float32
 BF16 = jnp.bfloat16
 PIECES = 4
-AHEAD = (13, 2)
+AHEAD = (12, 2, 2)
+MOVED_AT = 10.0
 PLACE_BYTES = 1024 * 1024
 VMEM_BYTES = 52 * 1024 * 1024
 (
@@ -28,16 +29,14 @@
     PROJ,
     HEAD,
     GATHER_Z,
-    GATHER_A,
-    GATHER_B,
+    GATHER_P,
     GATHER_C,
     SQUARE,
     SCALE,
     SUM_C,
-    SUM_Y,
-    SUM_X,
+    SUM_P,
     SUM_Z,
-) = range(18)
+) = range(16)
 
 
 def span(index, size):
@@ -55,22 +54,21 @@
 
 
 def schedule(zs):
-    Z, FIRST, SECOND, HALF, DENSE, EXPERT, DOWN, TWIN, HIDDEN, SUMS_Y, SUMS_X, SCALES, STATE = range(13)
-    cost = (0.05, 0.05, 0.08, 0.5, 0.4, 0.6, 0.4, 0.53, 0.05, 0.37, 0.05, 0.1, 2.6)
-    relays = (Z, FIRST, SECOND, SCALES, HIDDEN)
-    after = {(STATE, 0): [], (SCALES, 0): [(None, 2.8)]}
+    Z, PLANE, HALF, SECOND, DOWN, DENSE, TWIN, HIDDEN, ADD, SUMS, SCALES, STATE = range(12)
+    cost = (0.05, 0.08, 0.4, 0.55, 0.35, 0.55, 0.5, 0.05, 0.35, 0.05, 0.1, 2.1)
+    relays = (Z, PLANE, SCALES, HIDDEN)
+    after = {(STATE, 0): [], (SCALES, 0): [(None, 2.5)]}
     for k in range(zs):
         after[Z, k] = [(None, 2.8 + 1.6 * k if k else 0.0)]
-        after[FIRST, k] = [((Z, k), 2.5)]
-        after[SECOND, k] = [((FIRST, k), 2.5)]
-        after[HALF, k] = [((SECOND, k), 0.0)]
-        after[DENSE, k] = [((SECOND, k), 1.4), ((HALF, k), 0.0), ((SCALES, 0), 2.5)]
-        after[EXPERT, k] = [((DENSE, k), 0.0)]
-        after[DOWN, k] = [((EXPERT, k), 0.0)]
+        after[PLANE, k] = [((Z, k), 3.2)]
+        after[HALF, k] = [((PLANE, k), 0.0)]
+        after[SECOND, k] = [((PLANE, k), 1.4), ((HALF, k), 0.0), ((SCALES, 0), 2.5)]
+        after[DOWN, k] = [((SECOND, k), 0.0)]
+        after[DENSE, k] = [((SECOND, k), 0.0), (None, MOVED_AT)]
         after[TWIN, k] = [((DOWN, k), 1.4)]
-        after[HIDDEN, k] = [((DENSE, k), 2.6)]
-        after[SUMS_Y, k] = [((TWIN, k), 3.7), ((HIDDEN, k), 1.3)]
-        after[SUMS_X, k] = [((SUMS_Y, k), 2.7)]
+        after[HIDDEN, k] = [((DENSE, k), 4.0)]
+        after[ADD, k] = [((TWIN, k), 0.0), ((HIDDEN, k), 1.3)]
+        after[SUMS, k] = [((TWIN, k), 3.6), ((ADD, k), 2.9)]
     done, now, order = {(Z, 0): 0.0, None: 0.0}, 0.0, []
     del after[Z, 0]
     while after:
@@ -82,7 +80,7 @@
         now = max(now, min(ready.values()))
         step = min(
             (step for step, at in ready.items() if at <= now),
-            key=lambda step: (step[0] not in relays, step[0] == STATE, -step[0], step[1]),
+            key=lambda step: (step[0] not in relays, step[0] == STATE, step[0] in (ADD, TWIN), -step[0], step[1]),
         )
         now += cost[step[0]] + (0.8 if step == (DOWN, 0) else 0.0)
         done[step] = now
@@ -111,9 +109,6 @@
     wrap = xs * depth
     lanes = r.sqs.shape[1]
     half = sides * cols
-
-    def pick(first, second):
-        return first * (1 - c) + second * c
 
     def device(zz, xx, yy, cc):
         return {"ep": zz * xs + xx, "tp": yy * CORES + cc}
@@ -410,56 +405,45 @@
         total = total + r.hrecv[lax.rem(tp + tpn - s, tpn)].astype(F32)
     r.resid[...] = total
 
-    def block(zz, xx, yy, cc):
-        return r.rows.at[cc, span(zz * xs + xx, seq), span(yy, cols)]
-
-    r.rows[c, span(me, seq), span(y, cols)] = (total * r.gain2_v[:, mine]).astype(BF16)
-    own = block(z, x, y, c)
-    for k in far_first:
-        send(own, own, GATHER_Z, k, device(zat(k), x, y, c), z)
-
-    def plane(k, a, b):
-        xx = lax.rem(x + xs - pick(a, b), xs)
-        yy = lax.rem(y + sides - pick(b, a), sides)
-        return block(zat(k), xx, yy, c)
-
-    def forward_first(k):
-        ref = plane(k, 0, 0)
-        for q in range(1, sides):
-            peer = device(z, lax.rem(x + pick(q, 0), xs), lax.rem(y + pick(0, q), sides), c)
-            arrived[GATHER_A, k, q] = send(ref, ref, GATHER_A, k * sides + q, peer)
-
-    def forward_second(k, a):
-        ref = plane(k, a, 0)
-        for q in range(1, sides):
-            peer = device(z, lax.rem(x + pick(0, q), xs), lax.rem(y + pick(q, 0), sides), c)
-            arrived[GATHER_B, k, a, q] = send(
-                ref, ref, GATHER_B, (k * sides + a) * sides + q, peer
-            )
-
-    def forward_twin(k, a, b):
-        ref = plane(k, a, b)
-        arrived[GATHER_C, k, a, b] = send(
-            ref, ref, GATHER_C, (k * sides + a) * sides + b, device(z, x, y, twin_core)
-        )
-
-    forward_first(0)
-    forward_second(0, 0)
-    forward_twin(0, 0, 0)
-    move_pieces(len(pieces))
-
     square = to_row(jnp.sum(total * total, axis=-1, keepdims=True))
     r.sqs[...] = jnp.broadcast_to(square, (ROWS, lanes))
     for s in range(1, tpn):
         arrived[SQUARE, s] = send(
             r.sqs, r.sqr.at[tp], SQUARE, s, {"tp": lax.rem(tp + s, tpn)}
         )
+    def block(zz, xx, yy, cc):
+        return r.rows.at[cc, span(zz * xs + xx, seq), span(yy, cols)]
+
+    r.rows[c, span(me, seq), span(y, cols)] = (total * r.gain2_v[:, mine]).astype(BF16)
+    own = block(z, x, y, c)
+    for k in far_first:
+        send(own, own, GATHER_Z, k, device(zat(k), x, y, c), z)
+
+    offsets = [(a, b) for a in range(xs) for b in range(sides)]
+
+    def plane(k, a, b):
+        return block(zat(k), lax.rem(x + xs - a, xs), lax.rem(y + sides - b, sides), c)
+
+    def place(k, a, b):
+        return (k * xs + a) * sides + b
+
+    def forward_twin(k, a, b):
+        ref = plane(k, a, b)
+        arrived[GATHER_C, k, a, b] = send(
+            ref, ref, GATHER_C, place(k, a, b), device(z, x, y, twin_core)
+        )
+
+    def forward(k):
+        ref = plane(k, 0, 0)
+        for a, b in reversed(offsets[1:]):
+            peer = device(z, lax.rem(x + a, xs), lax.rem(y + b, sides), c)
+            arrived[GATHER_P, k, a, b] = send(ref, ref, GATHER_P, place(k, a, b), peer)
+        forward_twin(k, 0, 0)
+
+    forward(0)
+    move_pieces(AHEAD[2])
+
     size = xs * seq
-    pairs = [(r.egv, r.euv, e) for e in range(exp_local)] + [(r.dgv, r.duv, None)]
-
-    def weight(ref, lead, core):
-        return ref[core] if lead is None else ref[core, lead]
-
     def scale_out(k):
         square = r.sqs[:1]
         for s in range(1, tpn):
@@ -471,35 +455,23 @@
 
     def from_z(k):
         landed(GATHER_Z, zat(k), plane(k, 0, 0))
-        forward_first(k)
-        forward_second(k, 0)
-        forward_twin(k, 0, 0)
-
-    def from_first(k):
-        for a in range(1, sides):
-            arrived[GATHER_A, k, a].wait_recv()
-            forward_second(k, a)
-            forward_twin(k, a, 0)
-
-    def from_second(k):
-        for a in range(sides):
-            for b in range(1, sides):
-                arrived[GATHER_B, k, a, b].wait_recv()
-                forward_twin(k, a, b)
+        forward(k)
+        if k == zs - 1:
+            move_pieces(len(pieces))
+
+    def from_plane(k):
+        for a, b in offsets[1:]:
+            arrived[GATHER_P, k, a, b].wait_recv()
+            forward_twin(k, a, b)
 
     def first_half(k):
         if k == 0:
-            for copy in got.egv + got.dgv:
+            for copy in got.egv:
                 copy.wait()
-            moved()
         lhs = r.rows[c, span(zat(k), size), :]
-        for i, (gate, up, lead) in enumerate(pairs):
-            for j, ref in enumerate((gate, up)):
-                product = jnp.dot(lhs, weight(ref, lead, c), preferred_element_type=F32)
-                if lead is None:
-                    r.dacc[j, k] = product
-                else:
-                    r.acc[2 * i + j, k] = product
+        for i in range(exp_local):
+            for j, ref in enumerate((r.egv, r.euv)):
+                r.acc[2 * i + j, k] = jnp.dot(lhs, ref[c, i], preferred_element_type=F32)
 
     def column(ref, k, row):
         return jnp.concatenate(
@@ -532,10 +504,9 @@
             value = r.wide[...]
         return value
 
-    def dense_half(k):
-        for a in range(sides):
-            for b in range(sides):
-                arrived[GATHER_C, k, a, b].wait_recv()
+    def second_half(k):
+        for a, b in offsets:
+            arrived[GATHER_C, k, a, b].wait_recv()
         if k == 0:
             for s in range(1, n):
                 arrived[ROUTE, s].wait_recv()
@@ -543,43 +514,50 @@
             if k or i:
                 e = zat(k) * xs + lax.rem(x + i, xs)
                 landed(SCALE, e, r.scr.at[e])
-        hidden_of(k, len(pairs) - 1)
-
-    def expert_half(k):
-        for i in range(exp_local):
-            hidden_of(k, i)
-
-    def hidden_of(k, i):
         scale = column(r.scr, k, 0)
         lhs = r.rows[twin_core, span(zat(k), size), :]
-        gate, up, lead = pairs[i]
-        both = []
-        for j, ref in enumerate((gate, up)):
-            before = r.dacc[j, k] if lead is None else r.acc[2 * i + j, k]
-            product = jnp.dot(lhs, weight(ref, lead, twin_core), preferred_element_type=F32)
-            both.append(scale * (before + product))
-        hidden = silu(both[0]) * both[1]
-        if lead is None:
-            r.dhid[k, tp] = hidden.astype(BF16)
-            ref = r.dhid.at[k, tp]
-            for q in range(1, sides):
-                peer = device(z, x, lax.rem(y + q, sides), c)
-                arrived[HIDDEN_Y, k, q] = send(ref, ref, HIDDEN_Y, k * sides + q, peer)
-            arrived[HIDDEN_C, k, 0] = send(
-                ref, ref, HIDDEN_C, k * sides, device(z, x, y, twin_core)
+        for i in range(exp_local):
+            gate, up = [
+                scale
+                * (
+                    r.acc[2 * i + j, k]
+                    + jnp.dot(lhs, ref[twin_core, i], preferred_element_type=F32)
+                )
+                for j, ref in enumerate((r.egv, r.euv))
+            ]
+            share = column(r.rrecv, k, i)
+            r.hid[k, :, i * ff : (i + 1) * ff] = (silu(gate) * up * share).astype(BF16)
+
+    def dense_hidden(k):
+        if k == 0:
+            for copy in got.dgv:
+                copy.wait()
+            moved()
+        scale = column(r.scr, k, 0)
+        gate, up = [
+            scale
+            * sum(
+                jnp.dot(r.rows[i, span(zat(k), size), :], ref[i], preferred_element_type=F32)
+                for i in range(CORES)
             )
-        else:
-            share = column(r.rrecv, k, lead)
-            r.hid[k, :, i * ff : (i + 1) * ff] = (hidden * share).astype(BF16)
+            for ref in (r.dgv, r.duv)
+        ]
+        r.dhid[k, tp] = (silu(gate) * up).astype(BF16)
+        ref = r.dhid.at[k, tp]
+        for q in range(1, sides):
+            peer = device(z, x, lax.rem(y + q, sides), c)
+            arrived[HIDDEN_Y, k, q] = send(ref, ref, HIDDEN_Y, k * sides + q, peer)
+        arrived[HIDDEN_C, k, 0] = send(ref, ref, HIDDEN_C, k * sides, device(z, x, y, twin_core))
 
     def down(k):
         if k == 0:
             for copy in got.edv:
                 copy.wait()
             shared_expert()
+        for q in range(sides):
+            r.part[k * sides + q] = partial(k, lax.rem(y + q, sides), twin_core).astype(BF16)
         for q in [*range(1, sides), 0]:
             slot = k * sides + q
-            r.part[slot] = partial(k, lax.rem(y + q, sides), twin_core).astype(BF16)
             arrived[SUM_C, k, q] = send(
                 r.part.at[slot], r.crecv.at[slot], SUM_C, slot, device(z, x, y, twin_core)
             )
@@ -593,21 +571,24 @@
             )
 
     def from_twin(k):
+        values = [partial(k, lax.rem(y + q, sides), c) for q in range(sides)]
         for q in [*range(1, sides), 0]:
             slot = k * sides + q
-            yy = lax.rem(y + q, sides)
-            value = partial(k, yy, c)
             arrived[SUM_C, k, q].wait_recv()
-            value = value + r.crecv[slot].astype(F32)
+            value = values[q] + r.crecv[slot].astype(F32)
             if q == 0:
                 r.keep[k] = value
                 continue
             r.ysend[slot] = value.astype(BF16)
-            arrived[SUM_Y, k, q] = send(
-                r.ysend.at[slot], r.yrecv.at[slot], SUM_Y, slot, device(z, x, yy, c)
-            )
-
-    def from_y(k):
+            for j in range(xs):
+                sum_out(k, j, q, r.ysend.at[slot, span(lax.rem(x + j, xs), seq)])
+
+    def sum_out(k, j, q, ref):
+        peer = device(z, lax.rem(x + j, xs), lax.rem(y + q, sides), c)
+        at = place(k, j, q)
+        arrived[SUM_P, k, j, q] = send(ref, r.plane_sums.at[at], SUM_P, at, peer)
+
+    def add_dense(k):
         for q in range(sides):
             arrived[HIDDEN_C, k, q].wait_recv()
         if k == 0:
@@ -618,24 +599,18 @@
             )
             for t in range(tpn)
         )
-        value = r.keep[k] + jax.nn.sigmoid(r.mix_v[...]) * dense
-        for q in range(1, sides):
-            arrived[SUM_Y, k, q].wait_recv()
-            value = value + r.yrecv[k * sides + q].astype(F32)
-        r.keep[k] = value
-        for q in range(1, xs):
-            slot = k * sides + q
-            xx = lax.rem(x + q, xs)
-            r.xsend[slot] = r.keep[k, span(xx, seq), :].astype(BF16)
-            arrived[SUM_X, k, q] = send(
-                r.xsend.at[slot], r.xrecv.at[slot], SUM_X, slot, device(z, xx, y, c)
-            )
-
-    def from_x(k):
+        r.keep[k] = r.keep[k] + jax.nn.sigmoid(r.mix_v[...]) * dense
+        for j in range(1, xs):
+            slot = k * sides
+            rows_at = span(lax.rem(x + j, xs), seq)
+            r.ysend[slot, rows_at, :] = r.keep[k, rows_at, :].astype(BF16)
+            sum_out(k, j, 0, r.ysend.at[slot, rows_at])
+
+    def from_sums(k):
         value = r.keep[k, span(x, seq), :]
-        for q in range(1, xs):
-            arrived[SUM_X, k, q].wait_recv()
-            value = value + r.xrecv[k * sides + q].astype(F32)
+        for j, q in offsets[1:]:
+            arrived[SUM_P, k, j, q].wait_recv()
+            value = value + r.plane_sums[place(k, j, q)].astype(F32)
         if k == 0:
             r.resid[...] = r.resid[...] + value
         else:
@@ -646,8 +621,18 @@
         lax.fori_loop(0, groups, write_group, 0)
 
     kinds = (
-        from_z, from_first, from_second, first_half, dense_half, expert_half, down,
-        from_twin, hidden_on, from_y, from_x, scale_out, write_state,
+        from_z,
+        from_plane,
+        first_half,
+        second_half,
+        down,
+        dense_hidden,
+        from_twin,
+        hidden_on,
+        add_dense,
+        from_sums,
+        scale_out,
+        write_state,
     )
     for kind, k in schedule(zs):
         step = kinds[kind]
@@ -789,17 +774,14 @@
         duv=VM((CORES, half, dff), BF16),
         ddv=VM(dense_down.shape, BF16),
         acc=VM((2 * exp_local, zs, size, ff), F32),
-        dacc=VM((2, zs, size, dff), F32),
         hid=VM((zs, size, exp_local * ff), BF16),
         dhid=VM((zs, tpn, size, dff), BF16),
         wide=VM((size, cols), F32),
         part=VM((zs * sides, size, cols), BF16),
         crecv=VM((zs * sides, size, cols), BF16),
         ysend=VM((zs * sides, size, cols), BF16),
-        yrecv=VM((zs * sides, size, cols), BF16),
+        plane_sums=VM((hops, seq, cols), BF16),
         keep=VM((zs, size, cols), F32),
-        xsend=VM((zs * sides, seq, cols), BF16),
-        xrecv=VM((zs * sides, seq, cols), BF16),
         zsend=VM((zs, seq, cols), BF16),
         zrecv=VM((zs, seq, cols), BF16),
         shared=VM((tpn, seq, cols), F32),
@@ -815,14 +797,12 @@
         PROJ: 4 * zs,
         HEAD: tpn,
         GATHER_Z: zs,
-        GATHER_A: zs * sides,
-        GATHER_B: hops,
+        GATHER_P: hops,
         GATHER_C: hops,
         SQUARE: tpn,
         SCALE: n,
         SUM_C: zs * sides,
-        SUM_Y: zs * sides,
-        SUM_X: zs * sides,
+        SUM_P: hops,
         SUM_Z: zs,
     }
     names = [*ins, *outs, *scratch]

time: 70.3 us -> 68 us (0.967)
  Pallas kernels: 69.5 us -> 67.2 us
    pallas_call x1, Pallas kernels: 66.7 us -> 64.5 us  [local(): pl.pallas_call(functools.partial(layer_kernel, n, tpn, move, names), out_...]
where the time goes in v3:
time: 68 us; the launch traced here: 67.9 us
  Pallas kernels  67.2 us (99%)
    pallas_call x1, Pallas kernels, local(): pl.pallas_call(functools.partial(layer_kernel, n, tpn, move, names), out_...  64.5 us
    pallas_call x1, Pallas kernels, local(): pl.pallas_call(place_kernel, out_shape=tuple(outs.values()), in_specs=[pl...  2.73 us

profile of v3, /device:TPU:0, one launch (start us, length us, event | category | flops | bytes accessed | tf_op | source)
XLA Modules:
  0.0 67.9 jit_solution(8610703675494118447)
XLA Ops:
  0.6 64.5 %shard_map.230 = (bf16[48,512]{1,0:T(8,128)(2,1)S(1)}, f32[48,2,128,128]{3,2,1,0:T(8,128)S(1)}) custom-call(bf16[48,2048]{1,0:T(8,128)(2,1)} %refs_0_.1, f32[48,2,128,128]{3,2,1,0:T(8,128)} %refs_1_.1, f32[1,2048]{1,0:T(1,128)} %bitcast.7, bf16[256,256]{1,0:T(8,128)(2,1)} %refs_3_.1, bf16[256,256]{1,0:T(8,128)(2,1)} %refs_4_.1, bf16[256,256]{1,0:T(8,128)(2,1)} %refs_5_.1, ...), custom_call_target="tpu_custom_call" | custom-call | tf_op jit(solution)/shard_map/pallas_call | solution.py:810
  65.2 2.7 %shard_map.231 = (bf16[48,512]{1,0:T(8,128)(2,1)}, f32[48,2,128,128]{3,2,1,0:T(8,128)}) custom-call(bf16[48,512]{1,0:T(8,128)(2,1)S(1)} %get-tuple-element.4.held, f32[48,2,128,128]{3,2,1,0:T(8,128)S(1)} %get-tuple-element.5.held_state), custom_call_target="tpu_custom_call" | custom-call | tf_op jit(solution)/shard_map/pallas_call | solution.py:820

commit v4 on v3

--- a/solution.py
+++ b/solution.py
@@ -63,7 +63,7 @@
         after[PLANE, k] = [((Z, k), 3.2)]
         after[HALF, k] = [((PLANE, k), 0.0)]
         after[SECOND, k] = [((PLANE, k), 1.4), ((HALF, k), 0.0), ((SCALES, 0), 2.5)]
-        after[DOWN, k] = [((SECOND, k), 0.0)]
+        after[DOWN, k] = [((SECOND, k), 0.0), ((Z, zs - 1), 0.0)]
         after[DENSE, k] = [((SECOND, k), 0.0), (None, MOVED_AT)]
         after[TWIN, k] = [((DOWN, k), 1.4)]
         after[HIDDEN, k] = [((DENSE, k), 4.0)]

time: 68 us -> 68.4 us (level)
  no operation moved by 1% of the time
where the time goes in v4:
time: 68.4 us; the launch traced here: 68.3 us
  Pallas kernels  67.6 us (99%)
    pallas_call x1, Pallas kernels, local(): pl.pallas_call(functools.partial(layer_kernel, n, tpn, move, names), out_...  64.9 us
    pallas_call x1, Pallas kernels, local(): pl.pallas_call(place_kernel, out_shape=tuple(outs.values()), in_specs=[pl...  2.73 us

profile of v4, /device:TPU:0, one launch (start us, length us, event | category | flops | bytes accessed | tf_op | source)
XLA Modules:
  0.0 68.3 jit_solution(8672080833943403774)
XLA Ops:
  0.6 64.9 %shard_map.230 = (bf16[48,512]{1,0:T(8,128)(2,1)S(1)}, f32[48,2,128,128]{3,2,1,0:T(8,128)S(1)}) custom-call(bf16[48,2048]{1,0:T(8,128)(2,1)} %refs_0_.1, f32[48,2,128,128]{3,2,1,0:T(8,128)} %refs_1_.1, f32[1,2048]{1,0:T(1,128)} %bitcast.7, bf16[256,256]{1,0:T(8,128)(2,1)} %refs_3_.1, bf16[256,256]{1,0:T(8,128)(2,1)} %refs_4_.1, bf16[256,256]{1,0:T(8,128)(2,1)} %refs_5_.1, ...), custom_call_target="tpu_custom_call" | custom-call | tf_op jit(solution)/shard_map/pallas_call | solution.py:810
  65.5 2.7 %shard_map.231 = (bf16[48,512]{1,0:T(8,128)(2,1)}, f32[48,2,128,128]{3,2,1,0:T(8,128)}) custom-call(bf16[48,512]{1,0:T(8,128)(2,1)S(1)} %get-tuple-element.4.held, f32[48,2,128,128]{3,2,1,0:T(8,128)S(1)} %get-tuple-element.5.held_state), custom_call_target="tpu_custom_call" | custom-call | tf_op jit(solution)/shard_map/pallas_call | solution.py:820
